TPU v7x, 32 devices: a whole 2x2x4 slice. The times are simulated.
32 devices in a mesh: grp: 2 (over x), sp: 8 (over z, y), tp: 2 (over core).
Axes of the slice: x: 2, y: 2, z: 4, core: 2. Of those that a mesh axis runs over, the one named last changes fastest.
Arguments:
- tokens: bfloat16 [8192, 2048], P(('grp', 'sp', 'tp')), parts along dimension 0, may hold values from -60 to 60
- query_weight: bfloat16 [2048, 1024], P(None, 'tp'), may hold values from -0.125 to 0.125
- key_weight: bfloat16 [2048, 1024], P(None, 'tp'), may hold values from -0.125 to 0.125
- value_weight: bfloat16 [2048, 1024], P(None, 'tp'), may hold values from -0.125 to 0.125
- output_weight: bfloat16 [1024, 2048], P(None, 'tp'), may hold values from -1.5 to 1.5
Outputs:
- attended: bfloat16 [8192, 2048], P(('grp', 'sp'), 'tp'), parts along dimension 0
There are 2 independent parts, one for each index of `grp`. A program takes and returns all parts, laid end to end along the dimension named above; an argument that names none is the same for every part. Nothing has to cross between parts.
All inputs are finite; a program needn't handle non-finite values.
Results may differ from a plain program's by a relative error of at most 0.012.
The roundings to bfloat16 on the way count: a program that leaves them out, or rounds other values in their place, can miss the bound.
Values may be sent and summed in bfloat16 or wider, within the bound.
A program may use at most 128 MiB of HBM per device.

v0:
```python
import functools

import jax
import jax.numpy as jnp
import numpy as np
from jax import lax
from jax.experimental import pallas as pl
from jax.experimental.pallas import tpu as pltpu
from jax.sharding import PartitionSpec as P

HEAD = 128
REACH_STEPS = 128
MIDDLE_DILATION = 4
FAR_DILATION = 16
THETA_BASE = 500000.0
NEG = -1e30
MESH = pl.DeviceIdType.MESH
F32 = jnp.float32
BF16 = jnp.bfloat16

A, C, O = 0, 1, 2
SLOTS = 3
CLASSES = MIDDLE_DILATION
CLASS_ROWS = 128


def spot(i):
    return (i >> 6) * 256 + (i & 15) * 16 + ((i >> 4) & 3) * 4


def iota(shape, dim):
    return lax.broadcasted_iota(jnp.int32, shape, dim)


def rotated(x, cosine, sine):
    return x * cosine + pltpu.roll(x, HEAD // 2, 1) * sine


def softmax(scores, values):
    top = jnp.max(scores, axis=-1, keepdims=True)
    raised = jnp.exp(scores - top)
    total = jnp.sum(raised, axis=-1, keepdims=True)
    weights = (raised * (1.0 / total)).astype(BF16)
    result = jnp.dot(weights, values, preferred_element_type=F32)
    return result, top + jnp.log(total)


def transposed_dot(a, b):
    return lax.dot_general(a, b, (((1,), (1,)), ((), ())), preferred_element_type=F32)


def kernel(
    n_sp, heads,
    tok_hbm, wq_hbm, wk_hbm, wv_hbm, wo_hbm, inv_hbm,
    out_ref,
    tok, wkv, wq, wo, inv, cos_ref, sin_ref, xg, ctx, q, visitor, k1, v1, perm, unperm,
    b16, b4, b1, near_out, near_lse, part, part_lse, far_out, far_lse, mixp, mixg, out_sum,
    load_sem, x_sem, ctx_send, ctx_recv, q_sem, part_sem, lse_sem, mix_send, mix_recv,
):
    sp = lax.axis_index("sp")
    tp = lax.axis_index("tp")
    z = sp // 2
    odd = sp % 2
    even = odd == 0
    other = 1 - tp
    has_next = z + 1 < n_sp // 2

    tok_copy = pltpu.make_async_copy(tok_hbm, tok, load_sem.at[0])
    tok_copy.start()
    inv_copy = pltpu.make_async_copy(inv_hbm, inv, load_sem.at[2 + 2 * heads + heads // 2])
    inv_copy.start()
    kv_copies = []
    for h in range(heads):
        cols = pl.ds(h * HEAD, HEAD)
        pair = (
            pltpu.make_async_copy(wk_hbm.at[:, cols], wkv.at[h, :, pl.ds(0, HEAD)], load_sem.at[1 + 2 * h]),
            pltpu.make_async_copy(wv_hbm.at[:, cols], wkv.at[h, :, pl.ds(HEAD, HEAD)], load_sem.at[2 + 2 * h]),
        )
        for copy in pair:
            copy.start()
        kv_copies.append(pair)
    q_copies = []
    for p in range(heads // 2):
        copy = pltpu.make_async_copy(
            wq_hbm.at[:, pl.ds(p * 2 * HEAD, 2 * HEAD)], wq.at[p], load_sem.at[1 + 2 * heads + p])
        copy.start()
        q_copies.append(copy)
    wo_copy = pltpu.make_async_copy(wo_hbm, wo, load_sem.at[1 + 2 * heads + heads // 2])
    wo_copy.start()

    barrier = pltpu.get_barrier_semaphore()
    y_partner = sp + 1 - 2 * odd

    def greet(ids):
        pl.semaphore_signal(barrier, inc=1, device_id=ids, device_id_type=MESH)

    greet({"tp": other})
    greet({"sp": y_partner})

    @pl.when(has_next)
    def _():
        greet({"sp": sp + 2})

    @pl.when(z > 0)
    def _():
        greet({"sp": sp - 2})

    row = iota((256, 256), 0)
    perm[...] = jnp.where(spot(row & 63) + (row >> 6) == iota((256, 256), 1), 1.0, 0.0).astype(BF16)

    pl.semaphore_wait(barrier, 2 + has_next.astype(jnp.int32) + (z > 0).astype(jnp.int32))

    tok_copy.wait()
    width = tok.shape[1]

    def reorder(i, _):
        cols = pl.ds(pl.multiple_of(i * 512, 512), 512)
        moved = jnp.dot(perm[...], tok[:, cols], preferred_element_type=F32).astype(BF16)
        xg[:, tp, :, cols] = moved.reshape(CLASSES, 64, 512)
        return 0

    lax.fori_loop(0, width // 512, reorder, 0)
    x_copy = pltpu.make_async_remote_copy(
        src_ref=xg.at[:, tp], dst_ref=xg.at[:, tp], send_sem=x_sem.at[0], recv_sem=x_sem.at[1],
        device_id={"tp": other}, device_id_type=MESH)
    x_copy.start()

    inv_copy.wait()
    lane = iota((128, HEAD), 1)

    def table(c, _):
        positions = sp * 512 + spot(iota((128, HEAD), 0)) + c
        angles = positions.astype(F32) * inv[...]
        rows = pl.ds(pl.multiple_of(c * 128, 128), 128)
        cos_ref[rows, :] = jnp.cos(angles)
        sine = jnp.sin(angles)
        sin_ref[rows, :] = jnp.where(lane < HEAD // 2, -sine, sine)
        return 0

    lax.fori_loop(0, CLASSES, table, 0)

    def remote(src, dst, send_sem, recv_sem, ids):
        return pltpu.make_async_remote_copy(
            src_ref=src, dst_ref=dst, send_sem=send_sem, recv_sem=recv_sem,
            device_id=ids, device_id_type=MESH)

    down = {"sp": sp + 2}
    up = {"sp": sp - 2}
    side = {"sp": y_partner}

    def send(h, src, dst, ids):
        return remote(ctx.at[h, :, :, src], ctx.at[h, :, :, dst],
                      ctx_send.at[dst, h], ctx_recv.at[dst, h], ids)

    def send_own(h):
        return ((has_next, send(h, O, A, down)), (even, send(h, O, C, side)))

    def send_relay(h):
        return (((odd == 1) & (z > 0), send(h, A, C, side)),)

    def send_query(h):
        return ((z > 0, remote(q.at[h], visitor.at[h], q_sem.at[0, h], q_sem.at[1, h], up)),)

    def send_part(h):
        return ((has_next, remote(part.at[h], far_out.at[h], part_sem.at[0, h], part_sem.at[1, h], down)),
                (has_next, remote(part_lse.at[h], far_lse.at[h], lse_sem.at[0, h], lse_sem.at[1, h], down)))

    def start_all(sends):
        for condition, copy in sends:
            @pl.when(condition)
            def _():
                copy.start()

    def receive(h, slot):
        @pl.when(sp >= 2 - slot)
        def _():
            send(h, slot, slot, side).wait_recv()

    x_copy.wait_recv()

    def tokens():
        return xg[...].reshape(512, width)

    def project_kv(h, _):
        kv = jnp.dot(tokens(), wkv[h], preferred_element_type=F32)
        k = rotated(kv[:, :HEAD], cos_ref[...], sin_ref[...]).astype(BF16)
        ctx[h, 0, :, O] = k.reshape(CLASSES, 128, HEAD)
        ctx[h, 1, :, O] = kv[:, HEAD:].astype(BF16).reshape(CLASSES, 128, HEAD)
        start_all(send_own(h))
        return 0

    for pair in kv_copies:
        for copy in pair:
            copy.wait()
    lax.fori_loop(0, heads, project_kv, 0)

    for copy in q_copies:
        copy.wait()

    def project_q(p, _):
        qq = jnp.dot(tokens(), wq[p], preferred_element_type=F32)
        for s in range(2):
            r = rotated(qq[:, s * HEAD:(s + 1) * HEAD], cos_ref[...], sin_ref[...])
            q[2 * p + s] = r.astype(BF16).reshape(CLASSES, 128, HEAD)
            start_all(send_query(2 * p + s))
        return 0

    lax.fori_loop(0, heads // 2, project_q, 0)

    qi, kj = iota((128, 640), 0), iota((128, 640), 1)
    dist = 4 - (kj >> 7)
    diff = spot(qi) - spot(kj & 127) + 512 * dist
    here = (dist <= sp) | ((dist >= 3) & (dist <= sp + 2))
    far = here & ((diff & 15) == 0) & (diff >= 0) & (diff <= FAR_DILATION * REACH_STEPS)
    b16[...] = jnp.where(far, 0.0, NEG)
    mid = here & (diff >= 0) & (diff <= MIDDLE_DILATION * REACH_STEPS)
    b4[...] = jnp.where(mid, 0.0, NEG)[:, 384:]
    key_spot = jnp.where(kj < 128, kj - 128, spot(kj & 127) + ((kj >> 7) - 1))
    for c in range(CLASSES):
        near = spot(qi) + c - key_spot
        ok = (near >= 0) & (near <= REACH_STEPS) & ((kj >= 128) | (sp > 0))
        b1[c] = jnp.where(ok, 0.0, NEG)
    col = iota((512, 512), 1)
    unperm[...] = jnp.where(spot(col & 127) + (col >> 7) == iota((512, 512), 0), 1.0, 0.0).astype(BF16)

    for slot in (A, C):
        @pl.when(sp < 2 - slot)
        def _():
            def clear(h, _):
                ctx[h, :, :, slot] = jnp.zeros((2, CLASSES, 128, HEAD), BF16)
                return 0
            lax.fori_loop(0, heads, clear, 0)

    part_lse[...] = jnp.zeros(part_lse.shape, F32)

    @pl.when(z == 0)
    def _():
        far_out[...] = jnp.zeros(far_out.shape, BF16)
        far_lse[...] = jnp.full(far_lse.shape, NEG, F32)

    def mix_copy(h):
        cols = pl.ds(pl.multiple_of(h * HEAD, HEAD), HEAD)
        return pltpu.make_async_remote_copy(
            src_ref=mixg.at[tp, :, cols], dst_ref=mixg.at[tp, :, cols],
            send_sem=mix_send.at[h], recv_sem=mix_recv.at[h],
            device_id={"tp": other}, device_id_type=MESH)

    eye = iota((128, 128), 0) == iota((128, 128), 1)

    def visit(h):
        @pl.when(has_next)
        def _():
            remote(q.at[h], visitor.at[h], q_sem.at[0, h], q_sem.at[1, h], side).wait_recv()

            def of_class(c, _):
                keys = ctx[h, 0, c, A:O].reshape(2 * 128, HEAD)
                vals = ctx[h, 1, c, A:O].reshape(2 * 128, HEAD)
                scores = transposed_dot(visitor[h, c], keys) * HEAD ** (-0.5)
                result, lse = softmax(scores + b16[:, :256], vals)
                part[h, c] = result.astype(BF16)
                part_lse[h, pl.ds(c, 1), :] = jnp.sum(jnp.where(eye, lse, 0.0), axis=0, keepdims=True)
                return 0

            lax.fori_loop(0, CLASSES, of_class, 0)

        start_all(send_part(h))

    def attend(h):
        tail = unperm[384:512, :]
        for kv, near in ((0, k1), (1, v1)):
            last = ctx[h, kv, :, C].reshape(512, HEAD)
            near[0:128] = jnp.dot(tail, last, preferred_element_type=F32).astype(BF16)
            near[128:640] = ctx[h, kv, :, O].reshape(512, HEAD)

        def of_class(c, _):
            qc = q[h, c]
            keys = ctx[h, 0, c].reshape(SLOTS * 128, HEAD)
            vals = ctx[h, 1, c].reshape(SLOTS * 128, HEAD)
            scores = transposed_dot(qc, keys) * HEAD ** (-0.5)
            r16, l16 = softmax(scores + b16[:, 256:], vals)
            r4, l4 = softmax(scores[:, 128:] + b4[...], vals[128:])
            r1, l1 = softmax(transposed_dot(qc, k1[...]) * HEAD ** (-0.5) + b1[c], v1[...])
            most = jnp.maximum(jnp.maximum(l16, l4), l1)
            e16, e4, e1 = jnp.exp(l16 - most), jnp.exp(l4 - most), jnp.exp(l1 - most)
            total = e16 + e4 + e1
            share = 1.0 / total
            near_out[h, c] = r1 * (e1 * share) + r4 * (e4 * share) + r16 * (e16 * share)
            near_lse[h, c] = jnp.broadcast_to(most + jnp.log(total), (128, HEAD))
            return 0

        lax.fori_loop(0, CLASSES, of_class, 0)

    def step(h, _):
        @pl.when(h < heads)
        def _():
            receive(h, A)
            start_all(send_relay(h))

        @pl.when(h > 0)
        def _():
            receive(h - 1, C)
            visit(h - 1)

        @pl.when((h > 0) & (h < heads))
        def _():
            attend(h - 1)
        return 0

    lax.fori_loop(0, heads + 1, step, 0)

    def combine(h):
        @pl.when(z > 0)
        def _():
            remote(part.at[h], far_out.at[h], part_sem.at[0, h], part_sem.at[1, h], side).wait_recv()
            remote(part_lse.at[h], far_lse.at[h], lse_sem.at[0, h], lse_sem.at[1, h], side).wait_recv()

        for c in range(CLASSES):
            row = far_lse[h, c:c + 1, :]
            lf = jnp.sum(jnp.where(eye, row, 0.0), axis=1, keepdims=True)
            ln = near_lse[h, c]
            most = jnp.maximum(ln, lf)
            en, ef = jnp.exp(ln - most), jnp.exp(lf - most)
            mixed = (near_out[h, c] * en + far_out[h, c].astype(F32) * ef) / (en + ef)
            mixp[c * 128:(c + 1) * 128, :] = mixed.astype(BF16)
        natural = jnp.dot(unperm[...], mixp[...], preferred_element_type=F32).astype(BF16)
        cols = pl.ds(pl.multiple_of(h * HEAD, HEAD), HEAD)
        mixg[tp, :, cols] = natural
        mix_copy(h).start()

    def gathered(h, _):
        mix_copy(h).wait_recv()
        return 0

    half = mixg.shape[2]
    first = half // 2

    def partial_out(i, _):
        cols = pl.ds(pl.multiple_of(i * 256, 256), 256)
        total = jnp.dot(mixg[0, :, :first], wo[:first, cols], preferred_element_type=F32)
        total = total + jnp.dot(mixg[1, :, :first], wo[half:half + first, cols], preferred_element_type=F32)
        out_sum[:, cols] = total
        return 0

    def finish(h, _):
        @pl.when(h == heads - 2)
        def _():
            attend(heads - 1)

        @pl.when(h == heads - 1)
        def _():
            wo_copy.wait()
            lax.fori_loop(0, heads // 2, gathered, 0)
            lax.fori_loop(0, out_ref.shape[1] // 256, partial_out, 0)

        combine(h)
        return 0

    lax.fori_loop(0, heads, finish, 0)

    lax.fori_loop(heads // 2, heads, gathered, 0)

    def project_out(i, _):
        cols = pl.ds(pl.multiple_of(i * 256, 256), 256)
        total = jnp.dot(mixg[0, :, first:], wo[first:half, cols], preferred_element_type=F32)
        total = total + jnp.dot(mixg[1, :, first:], wo[half + first:, cols], preferred_element_type=F32)
        out_ref[:, cols] = (out_sum[:, cols] + total).astype(BF16)
        return 0

    lax.fori_loop(0, out_ref.shape[1] // 256, project_out, 0)

    x_copy.wait_send()

    def left(h, _):
        for sends in (send_own(h), send_relay(h), send_query(h), send_part(h)):
            for condition, copy in sends:
                @pl.when(condition)
                def _():
                    copy.wait_send()
        mix_copy(h).wait_send()
        return 0

    lax.fori_loop(0, heads, left, 0)


def body(tokens, query_weight, key_weight, value_weight, output_weight):
    n_sp = lax.axis_size("sp")
    half_rows, width = tokens.shape
    rows = half_rows * lax.axis_size("tp")
    heads = query_weight.shape[1] // HEAD
    assert rows * 4 == FAR_DILATION * REACH_STEPS and rows == 512
    assert n_sp % 2 == 0 and lax.axis_size("tp") == 2 and heads % 2 == 0 and heads >= 4

    half = HEAD // 2
    inverse = THETA_BASE ** (-np.arange(half, dtype=np.float64) / half)
    inverse = np.concatenate([inverse, inverse]).astype(np.float32)[None, :]

    anywhere = pl.BlockSpec(memory_space=pl.ANY)
    vmem = pl.BlockSpec(memory_space=pltpu.VMEM)
    out_cols = output_weight.shape[1]
    return pl.pallas_call(
        functools.partial(kernel, n_sp, heads),
        out_shape=jax.ShapeDtypeStruct((rows, out_cols), BF16),
        in_specs=[anywhere] * 6,
        out_specs=vmem,
        scratch_shapes=[
            pltpu.VMEM((half_rows, width), BF16),
            pltpu.VMEM((heads, width, 2 * HEAD), BF16),
            pltpu.VMEM((heads // 2, width, 2 * HEAD), BF16),
            pltpu.VMEM(output_weight.shape, BF16),
            pltpu.VMEM((1, HEAD), F32),
            pltpu.VMEM((rows, HEAD), F32),
            pltpu.VMEM((rows, HEAD), F32),
            pltpu.VMEM((CLASSES, 2, 64, width), BF16),
            pltpu.VMEM((heads, 2, CLASSES, SLOTS, 128, HEAD), BF16),
            pltpu.VMEM((heads, CLASSES, 128, HEAD), BF16),
            pltpu.VMEM((heads, CLASSES, 128, HEAD), BF16),
            pltpu.VMEM((640, HEAD), BF16),
            pltpu.VMEM((640, HEAD), BF16),
            pltpu.VMEM((256, 256), BF16),
            pltpu.VMEM((512, 512), BF16),
            pltpu.VMEM((128, 640), F32),
            pltpu.VMEM((128, 256), F32),
            pltpu.VMEM((CLASSES, 128, 640), F32),
            pltpu.VMEM((heads, CLASSES, 128, HEAD), F32),
            pltpu.VMEM((heads, CLASSES, 128, HEAD), F32),
            pltpu.VMEM((heads, CLASSES, 128, HEAD), BF16),
            pltpu.VMEM((heads, 8, 128), F32),
            pltpu.VMEM((heads, CLASSES, 128, HEAD), BF16),
            pltpu.VMEM((heads, 8, 128), F32),
            pltpu.VMEM((512, HEAD), BF16),
            pltpu.VMEM((2, rows, heads * HEAD), BF16),
            pltpu.VMEM((rows, out_cols), F32),
            pltpu.SemaphoreType.DMA((3 + 2 * heads + heads // 2,)),
            pltpu.SemaphoreType.DMA((2,)),
            pltpu.SemaphoreType.DMA((2, heads)),
            pltpu.SemaphoreType.DMA((2, heads)),
            pltpu.SemaphoreType.DMA((2, heads)),
            pltpu.SemaphoreType.DMA((2, heads)),
            pltpu.SemaphoreType.DMA((2, heads)),
            pltpu.SemaphoreType.DMA((heads,)),
            pltpu.SemaphoreType.DMA((heads,)),
        ],
        compiler_params=pltpu.CompilerParams(
            collective_id=0, has_side_effects=True, vmem_limit_bytes=63 * 1024 * 1024
        ),
    )(tokens, query_weight, key_weight, value_weight, output_weight, jnp.asarray(inverse))


def solution(mesh):
    in_specs = (
        P(("grp", "sp", "tp"), None),
        P(None, "tp"),
        P(None, "tp"),
        P(None, "tp"),
        P(None, "tp"),
    )
    out_specs = P(("grp", "sp"), "tp")
    return jax.shard_map(body, mesh=mesh, in_specs=in_specs, out_specs=out_specs, check_vma=False)
```

profile of v0, /device:TPU:11, one launch (start us, length us, event | category | flops | bytes accessed | tf_op | source)
XLA Modules:
  0.0 54.9 jit_solution(14728148728564380338)
XLA Ops:
  0.0 52.7 %shard_map.64 = bf16[512,1024]{1,0:T(8,128)(2,1)} custom-call(bf16[256,2048]{1,0:T(8,128)(2,1)} %tok_hbm.1, bf16[2048,512]{1,0:T(8,128)(2,1)} %wq_hbm.1, bf16[2048,512]{1,0:T(8,128)(2,1)} %wk_hbm.1, bf16[2048,512]{1,0:T(8,128)(2,1)} %wv_hbm.1, bf16[1024,1024]{1,0:T(8,128)(2,1)} %wo_hbm.1, f32[1,128]{1,0:T(1,128)} %constant.2.clone.inv_hbm), custom_call_target="tpu_custom_call" | custom-call | tf_op jit(solution)/shard_map/pallas_call | solution.py:400
  52.7 2.3 %copy.8 = bf16[512,1024]{1,0:T(8,128)(2,1)} copy(bf16[512,1024]{1,0:T(8,128)(2,1)} %shard_map.64) | data formatting | bytes 2097152
where the time goes:
time: 55.1 us; the launch traced here: 54.9 us
  Pallas kernels  52.7 us (96%)
  local copies, waits for them, and re-layouts  2.26 us (4%)
    pallas_call x1, Pallas kernels, body(): pl.pallas_call(functools.partial(kernel, n_sp, heads), out_shape=jax.Shap...  52.7 us
    unnamed x1, local copies, waits for them, and re-layouts  2.26 us

commit v1 on v0

--- a/solution.py
+++ b/solution.py
@@ -399,7 +399,7 @@
     out_cols = output_weight.shape[1]
     return pl.pallas_call(
         functools.partial(kernel, n_sp, heads),
-        out_shape=jax.ShapeDtypeStruct((rows, out_cols), BF16),
+        out_shape=pltpu.VMEM((rows, out_cols), BF16),
         in_specs=[anywhere] * 6,
         out_specs=vmem,
         scratch_shapes=[
@@ -441,7 +441,7 @@
             pltpu.SemaphoreType.DMA((heads,)),
         ],
         compiler_params=pltpu.CompilerParams(
-            collective_id=0, has_side_effects=True, vmem_limit_bytes=63 * 1024 * 1024
+            collective_id=0, has_side_effects=True, vmem_limit_bytes=56 * 1024 * 1024
         ),
     )(tokens, query_weight, key_weight, value_weight, output_weight, jnp.asarray(inverse))
 

time: 55.1 us -> 52.8 us (0.958)
  local copies, waits for them, and re-layouts: 2.26 us -> 0.97 us
  Pallas kernels: 52.7 us -> 51.7 us
    unnamed x1, local copies, waits for them, and re-layouts: 2.26 us -> 0.97 us
    pallas_call x1, Pallas kernels: 52.7 us -> 51.7 us  [body(): pl.pallas_call(functools.partial(kernel, n_sp, heads), out_shape=pltpu.VM...]
where the time goes in v1:
time: 52.8 us; the launch traced here: 52.7 us
  Pallas kernels  51.7 us (98%)
  local copies, waits for them, and re-layouts  0.97 us (2%)
    pallas_call x1, Pallas kernels, body(): pl.pallas_call(functools.partial(kernel, n_sp, heads), out_shape=pltpu.VM...  51.7 us

profile of v1, /device:TPU:11, one launch (start us, length us, event | category | flops | bytes accessed | tf_op | source)
XLA Modules:
  0.0 52.7 jit_solution(15253184337406472469)
XLA Ops:
  0.0 51.7 %shard_map.64 = bf16[512,1024]{1,0:T(8,128)(2,1)S(1)} custom-call(bf16[256,2048]{1,0:T(8,128)(2,1)} %tok_hbm.1, bf16[2048,512]{1,0:T(8,128)(2,1)} %wq_hbm.1, bf16[2048,512]{1,0:T(8,128)(2,1)} %wk_hbm.1, bf16[2048,512]{1,0:T(8,128)(2,1)} %wv_hbm.1, bf16[1024,1024]{1,0:T(8,128)(2,1)} %wo_hbm.1, f32[1,128]{1,0:T(1,128)} %constant.2.clone.inv_hbm), custom_call_target="tpu_custom_call" | custom-call | tf_op jit(solution)/shard_map/pallas_call | solution.py:400
  51.7 1.0 %copy.8 = bf16[512,1024]{1,0:T(8,128)(2,1)} copy(bf16[512,1024]{1,0:T(8,128)(2,1)S(1)} %shard_map.64) | data formatting | bytes 2097152

commit v2 on v1

v2 whole, which is shorter than its diff:
```python
import functools

import jax
import jax.numpy as jnp
import numpy as np
from jax import lax
from jax.experimental import pallas as pl
from jax.experimental.pallas import tpu as pltpu
from jax.sharding import PartitionSpec as P

HEAD = 128
REACH_STEPS = 128
MIDDLE_DILATION = 4
FAR_DILATION = 16
THETA_BASE = 500000.0
NEG = -1e30
MESH = pl.DeviceIdType.MESH
F32 = jnp.float32
BF16 = jnp.bfloat16
SCALE = HEAD ** -0.5 / float(np.log(2.0))

A, C, O = 0, 1, 2
SLOTS = 3
CLASSES = MIDDLE_DILATION
PIECES = 2


def iota(shape, dim):
    return lax.broadcasted_iota(jnp.int32, shape, dim)


def rotated(x, cosine, sine):
    return x * cosine + pltpu.roll(x, HEAD // 2, 1) * sine


def weighed(scores, values):
    top = jnp.max(scores, axis=-1, keepdims=True)
    raised = jnp.exp2(scores - top).astype(BF16)
    ones = jnp.ones(values.shape, BF16)
    both = jnp.dot(raised, jnp.concatenate([values, ones], axis=1), preferred_element_type=F32)
    return both[:, :HEAD], both[:, HEAD:], top


def transposed_dot(a, b):
    return lax.dot_general(a, b, (((1,), (1,)), ((), ())), preferred_element_type=F32)


def classed(start, count, c):
    return pl.ds(start + c, count, stride=CLASSES)


def kernel(
    n_sp, heads,
    tok_hbm, wq_hbm, wk_hbm, wv_hbm, wo_hbm, inv_hbm,
    out_ref,
    x, wkv, wq, wo, inv, cos_ref, sin_ref, ctx, q, qn, kn, vn, visitor, flat_a, flat_b,
    far_bias, visit_bias, band, num, tot, top, cnum, ctot, ctop,
    part, part_lse, far_out, far_lse, mixf, mixg, out_sum,
    tok_sem, kv_sem, q_load, wo_sem, inv_sem, x_send, x_recv,
    ctx_send, ctx_recv, q_sem, part_sem, lse_sem, mix_send, mix_recv,
):
    sp = lax.axis_index("sp")
    tp = lax.axis_index("tp")
    z = sp // 2
    odd = sp % 2
    even = odd == 0
    other = 1 - tp
    has_next = z + 1 < n_sp // 2
    half_rows = x.shape[1]
    rows = 2 * half_rows
    class_rows = rows // CLASSES
    half_class = class_rows // 2
    piece = half_rows // PIECES
    order = (tp, other)

    tok_copies = []
    for i in range(PIECES):
        span = pl.ds(i * piece, piece)
        copy = pltpu.make_async_copy(tok_hbm.at[span], x.at[tp, span], tok_sem.at[i])
        copy.start()
        tok_copies.append(copy)
    inv_copy = pltpu.make_async_copy(inv_hbm, inv, inv_sem.at[0])
    inv_copy.start()

    def kv_copy(h, kind):
        source = (wk_hbm, wv_hbm)[kind]
        cols = pl.ds(h * HEAD, HEAD)
        return pltpu.make_async_copy(source.at[:, cols], wkv.at[h, :, pl.ds(kind * HEAD, HEAD)], kv_sem.at[kind, h])

    for h in range(heads):
        for kind in range(2):
            kv_copy(h, kind).start()
    q_copies = []
    for p in range(heads // 2):
        copy = pltpu.make_async_copy(wq_hbm.at[:, pl.ds(p * 2 * HEAD, 2 * HEAD)], wq.at[p], q_load.at[p])
        copy.start()
        q_copies.append(copy)
    wo_copies = []
    for h in range(heads):
        for t in range(2):
            copy = pltpu.make_async_copy(
                wo_hbm.at[pl.ds((t * heads + h) * HEAD, HEAD)], wo.at[pl.ds((2 * h + t) * HEAD, HEAD)], wo_sem.at[t, h])
            copy.start()
            wo_copies.append(copy)

    barrier = pltpu.get_barrier_semaphore()
    y_partner = sp + 1 - 2 * odd

    def greet(ids):
        pl.semaphore_signal(barrier, inc=1, device_id=ids, device_id_type=MESH)

    greet({"tp": other})
    greet({"sp": y_partner})

    @pl.when(has_next)
    def _():
        greet({"sp": sp + 2})

    @pl.when(z > 0)
    def _():
        greet({"sp": sp - 2})

    def remote(src, dst, send_sem, recv_sem, ids):
        return pltpu.make_async_remote_copy(
            src_ref=src, dst_ref=dst, send_sem=send_sem, recv_sem=recv_sem,
            device_id=ids, device_id_type=MESH)

    down = {"sp": sp + 2}
    up = {"sp": sp - 2}
    side = {"sp": y_partner}
    across = {"tp": other}

    block = REACH_STEPS
    qi, kj = iota((block, SLOTS * block), 0), iota((block, SLOTS * block), 1)
    dist = O - kj // block
    steps = qi - (kj % block) + block * dist
    here = dist <= sp
    ratio = FAR_DILATION // MIDDLE_DILATION
    mid = here & (steps >= 0) & (steps <= REACH_STEPS)
    far = here & (steps >= 0) & (steps % ratio == 0) & (steps <= ratio * REACH_STEPS)
    far_bias[...] = jnp.where(mid & far, 1.0, jnp.where(mid | far, 0.0, NEG))
    older = steps[:, :2 * block] + 2 * block
    seen = here[:, :2 * block] & (older % ratio == 0) & (older <= ratio * REACH_STEPS)
    visit_bias[...] = jnp.where(seen, 0.0, NEG)
    ni, nj = iota((block, 2 * block), 0), iota((block, 2 * block), 1)
    gap = ni + block - nj
    band[1] = jnp.where((gap >= 0) & (gap <= REACH_STEPS), 0.0, NEG)
    share = block // CLASSES
    tail_gap = ni + block - ((nj % share) * CLASSES + nj // share)
    gap = jnp.where(nj < block, tail_gap, gap)
    band[0] = jnp.where((gap >= 0) & (gap <= REACH_STEPS) & ((nj >= block) | (sp > 0)), 0.0, NEG)

    for slot in (A, C):
        @pl.when(sp < 2 - slot)
        def _():
            def clear(h, _):
                ctx[h, :, :, slot] = jnp.zeros((2, CLASSES, class_rows, HEAD), BF16)
                return 0
            lax.fori_loop(0, heads, clear, 0)

    part_lse[...] = jnp.zeros(part_lse.shape, F32)

    @pl.when(z == 0)
    def _():
        far_out[...] = jnp.zeros(far_out.shape, BF16)
        far_lse[...] = jnp.full(far_lse.shape, NEG, F32)

    lane = iota((piece, HEAD), 1)

    def table(c, _):
        start = pl.multiple_of(c * piece, piece)
        positions = sp * rows + start + iota((piece, HEAD), 0)
        angles = positions.astype(F32) * inv[...]
        span = pl.ds(start, piece)
        cos_ref[span, :] = jnp.cos(angles)
        sine = jnp.sin(angles)
        sin_ref[span, :] = jnp.where(lane < HEAD // 2, -sine, sine)
        return 0

    inv_copy.wait()
    lax.fori_loop(tp * PIECES, tp * PIECES + PIECES, table, 0)

    pl.semaphore_wait(barrier, 2 + has_next.astype(jnp.int32) + (z > 0).astype(jnp.int32))

    def x_copy(i):
        span = pl.ds(i * piece, piece)
        return remote(x.at[tp, span], x.at[tp, span], x_send.at[i], x_recv.at[i], across)

    for i in range(PIECES):
        tok_copies[i].wait()
        x_copy(i).start()

    def send(h, half, src, dst, ids):
        spots = pl.ds(pl.multiple_of(half * half_class, half_class), half_class)
        return remote(ctx.at[h, :, :, src, spots], ctx.at[h, :, :, dst, spots],
                      ctx_send.at[dst, h, half], ctx_recv.at[dst, h, half], ids)

    def send_own(h, half):
        return ((has_next, send(h, half, O, A, down)), (even, send(h, half, O, C, side)))

    def send_relay(h, half):
        return (((odd == 1) & (z > 0), send(h, half, A, C, side)),)

    def send_query(h):
        return ((z > 0, remote(q.at[h], visitor.at[h], q_sem.at[0, h], q_sem.at[1, h], up)),)

    def send_part(h):
        return ((has_next, remote(part.at[h], far_out.at[h], part_sem.at[0, h], part_sem.at[1, h], down)),
                (has_next, remote(part_lse.at[h], far_lse.at[h], lse_sem.at[0, h], lse_sem.at[1, h], down)))

    def start_all(sends):
        for condition, copy in sends:
            @pl.when(condition)
            def _():
                copy.start()

    def project_kv(h, half):
        if half is None:
            source, natural, span = x[...].reshape(rows, x.shape[2]), pl.ds(0, rows), (0, rows)
            spots = pl.ds(0, class_rows)
        else:
            source, natural = x[half], pl.ds(pl.multiple_of(half * half_rows, half_rows), half_rows)
            span, spots = (0, half_rows), pl.ds(pl.multiple_of(half * half_class, half_class), half_class)
        kv = jnp.dot(source, wkv[h], preferred_element_type=F32)
        k = rotated(kv[:, :HEAD], cos_ref[natural], sin_ref[natural])
        v = kv[:, HEAD:]
        flat_a[span[0]:span[1]] = k
        flat_b[span[0]:span[1]] = v
        kn[h, natural] = k.astype(BF16)
        vn[h, natural] = v.astype(BF16)
        count = span[1] // CLASSES
        for c in range(CLASSES):
            ctx[h, 0, c, O, spots] = flat_a[classed(0, count, c), :].astype(BF16)
            ctx[h, 1, c, O, spots] = flat_b[classed(0, count, c), :].astype(BF16)
        for part_half in (order if half is None else (half,)):
            start_all(send_own(h, part_half))

    kv_copy(0, 0).wait()
    kv_copy(0, 1).wait()
    project_kv(0, tp)
    lax.fori_loop(other * PIECES, other * PIECES + PIECES, table, 0)
    for i in range(PIECES):
        x_copy(i).wait_recv()
    project_kv(0, other)

    def project_rest(h, _):
        kv_copy(h, 0).wait()
        kv_copy(h, 1).wait()
        project_kv(h, None)
        return 0

    lax.fori_loop(1, heads, project_rest, 0)

    for copy in q_copies:
        copy.wait()

    def project_q(p, _):
        qq = jnp.dot(x[...].reshape(rows, x.shape[2]), wq[p], preferred_element_type=F32)
        for s, flat in ((0, flat_a), (1, flat_b)):
            r = rotated(qq[:, s * HEAD:(s + 1) * HEAD], cos_ref[...], sin_ref[...])
            flat[...] = r
            qn[2 * p + s] = r.astype(BF16)
            for c in range(CLASSES):
                q[2 * p + s, c] = flat[classed(0, class_rows, c), :].astype(BF16)
            start_all(send_query(2 * p + s))
        return 0

    lax.fori_loop(0, heads // 2, project_q, 0)

    def near(h, b, keys, vals, bias):
        scores = transposed_dot(qn[h, b * block:(b + 1) * block], keys) * SCALE + bias
        n, t, m = weighed(scores, vals)
        span = pl.ds(pl.multiple_of(h * rows, rows) + b * block, block)
        num[span, :] = n
        tot[span, :] = t
        top[span, :] = jnp.broadcast_to(m, (block, HEAD))

    def near_inner(h, _):
        for b in range(1, rows // block):
            span = slice((b - 1) * block, (b + 1) * block)
            near(h, b, kn[h, span], vn[h, span], band[1])
        return 0

    def poll(h, half):
        @pl.when((odd == 1) & (z > 0))
        def _():
            send(h, half, A, A, side).wait_recv()
        start_all(send_relay(h, half))

    poll(0, tp)
    lax.fori_loop(0, heads // 2, near_inner, 0)
    poll(0, other)
    lax.fori_loop(heads // 2, heads, near_inner, 0)

    def mix_copy(h):
        cols = pl.ds(pl.multiple_of((2 * h + tp) * HEAD, HEAD), HEAD)
        return remote(mixg.at[:, cols], mixg.at[:, cols], mix_send.at[h], mix_recv.at[h], across)

    eye = iota((block, block), 0) == iota((block, block), 1)

    def visit(h):
        @pl.when(has_next)
        def _():
            remote(q.at[h], visitor.at[h], q_sem.at[0, h], q_sem.at[1, h], side).wait_recv()
            for c in range(CLASSES):
                keys = ctx[h, 0, c, A:O].reshape(2 * class_rows, HEAD)
                vals = ctx[h, 1, c, A:O].reshape(2 * class_rows, HEAD)
                n, t, m = weighed(transposed_dot(visitor[h, c], keys) * SCALE + visit_bias[...], vals)
                part[h, c] = (n / t).astype(BF16)
                lse = m + jnp.log2(t)
                part_lse[h, c:c + 1, :] = jnp.sum(jnp.where(eye, lse, 0.0), axis=0, keepdims=True)

        start_all(send_part(h))

    def attend(h):
        tails = [jnp.concatenate([ctx[h, kind, c, C, class_rows - share:] for c in range(CLASSES)] + [nat[h, :block]], axis=0)
                 for kind, nat in ((0, kn), (1, vn))]
        near(h, 0, tails[0], tails[1], band[0])
        for c in range(CLASSES):
            keys = ctx[h, 0, c].reshape(SLOTS * class_rows, HEAD)
            vals = ctx[h, 1, c].reshape(SLOTS * class_rows, HEAD)
            n, t, m = weighed(transposed_dot(q[h, c], keys) * SCALE + far_bias[...], vals)
            span = classed(pl.multiple_of(h * rows, rows), class_rows, c)
            near_top = top[span, :]
            most = jnp.maximum(near_top, m)
            old, new = jnp.exp2(near_top - most), jnp.exp2(m - most)
            cnum[h, c] = num[span, :] * old + n * new
            ctot[h, c] = tot[span, :] * old + t * new
            ctop[h, c] = most

    def step(h, _):
        for half in order:
            @pl.when(even & (z > 0))
            def _():
                send(h, half, A, A, side).wait_recv()

            @pl.when(sp > 0)
            def _():
                send(h, half, C, C, side).wait_recv()
        visit(h)

        @pl.when(h + 1 < heads)
        def _():
            poll(h + 1, tp)
        attend(h)

        @pl.when(h + 1 < heads)
        def _():
            poll(h + 1, other)
        return 0

    lax.fori_loop(0, heads, step, 0)

    def combine(h, _):
        @pl.when(z > 0)
        def _():
            remote(part.at[h], far_out.at[h], part_sem.at[0, h], part_sem.at[1, h], side).wait_recv()
            remote(part_lse.at[h], far_lse.at[h], lse_sem.at[0, h], lse_sem.at[1, h], side).wait_recv()

        for c in range(CLASSES):
            lf = jnp.sum(jnp.where(eye, far_lse[h, c:c + 1, :], 0.0), axis=1, keepdims=True)
            ln = ctop[h, c]
            most = jnp.maximum(ln, lf)
            en, ef = jnp.exp2(ln - most), jnp.exp2(lf - most)
            mixed = (cnum[h, c] * en + far_out[h, c].astype(F32) * ef) / (ctot[h, c] * en + ef)
            mixf[classed(0, class_rows, c), :] = mixed
        cols = pl.ds(pl.multiple_of((2 * h + tp) * HEAD, HEAD), HEAD)
        mixg[:, cols] = mixf[...].astype(BF16)
        mix_copy(h).start()
        return 0

    def gathered(h, _):
        mix_copy(h).wait_recv()
        return 0

    lax.fori_loop(0, heads - 1, combine, 0)
    for copy in wo_copies:
        copy.wait()
    lax.fori_loop(0, heads - 1, gathered, 0)
    most_in = (heads - 1) * 2 * HEAD

    def partial_out(i, _):
        cols = pl.ds(pl.multiple_of(i * 256, 256), 256)
        out_sum[:, cols] = jnp.dot(mixg[:, :most_in], wo[:most_in, cols], preferred_element_type=F32)
        return 0

    lax.fori_loop(0, out_ref.shape[1] // 256, partial_out, 0)
    combine(heads - 1, 0)
    gathered(heads - 1, 0)

    def project_out(i, _):
        cols = pl.ds(pl.multiple_of(i * 256, 256), 256)
        last = jnp.dot(mixg[:, most_in:], wo[most_in:, cols], preferred_element_type=F32)
        out_ref[:, cols] = (out_sum[:, cols] + last).astype(BF16)
        return 0

    lax.fori_loop(0, out_ref.shape[1] // 256, project_out, 0)

    for i in range(PIECES):
        x_copy(i).wait_send()

    def left(h, _):
        sends = send_query(h) + send_part(h)
        for half in range(2):
            sends = sends + send_own(h, half) + send_relay(h, half)
        for condition, copy in sends:
            @pl.when(condition)
            def _():
                copy.wait_send()
        mix_copy(h).wait_send()
        return 0

    lax.fori_loop(0, heads, left, 0)


def body(tokens, query_weight, key_weight, value_weight, output_weight):
    n_sp = lax.axis_size("sp")
    half_rows, width = tokens.shape
    rows = half_rows * lax.axis_size("tp")
    heads = query_weight.shape[1] // HEAD
    assert rows * 4 == FAR_DILATION * REACH_STEPS and rows == 512
    assert n_sp % 2 == 0 and lax.axis_size("tp") == 2 and heads % 2 == 0 and heads >= 4

    half = HEAD // 2
    inverse = THETA_BASE ** (-np.arange(half, dtype=np.float64) / half)
    inverse = np.concatenate([inverse, inverse]).astype(np.float32)[None, :]

    class_rows = rows // CLASSES
    anywhere = pl.BlockSpec(memory_space=pl.ANY)
    vmem = pl.BlockSpec(memory_space=pltpu.VMEM)
    out_cols = output_weight.shape[1]
    dma = pltpu.SemaphoreType.DMA
    return pl.pallas_call(
        functools.partial(kernel, n_sp, heads),
        out_shape=pltpu.VMEM((rows, out_cols), BF16),
        in_specs=[anywhere] * 6,
        out_specs=vmem,
        scratch_shapes=[
            pltpu.VMEM((2, half_rows, width), BF16),
            pltpu.VMEM((heads, width, 2 * HEAD), BF16),
            pltpu.VMEM((heads // 2, width, 2 * HEAD), BF16),
            pltpu.VMEM(output_weight.shape, BF16),
            pltpu.VMEM((1, HEAD), F32),
            pltpu.VMEM((rows, HEAD), F32),
            pltpu.VMEM((rows, HEAD), F32),
            pltpu.VMEM((heads, 2, CLASSES, SLOTS, class_rows, HEAD), BF16),
            pltpu.VMEM((heads, CLASSES, class_rows, HEAD), BF16),
            pltpu.VMEM((heads, rows, HEAD), BF16),
            pltpu.VMEM((heads, rows, HEAD), BF16),
            pltpu.VMEM((heads, rows, HEAD), BF16),
            pltpu.VMEM((heads, CLASSES, class_rows, HEAD), BF16),
            pltpu.VMEM((rows, HEAD), F32),
            pltpu.VMEM((rows, HEAD), F32),
            pltpu.VMEM((REACH_STEPS, SLOTS * REACH_STEPS), F32),
            pltpu.VMEM((REACH_STEPS, 2 * REACH_STEPS), F32),
            pltpu.VMEM((2, REACH_STEPS, 2 * REACH_STEPS), F32),
            pltpu.VMEM((heads * rows, HEAD), F32),
            pltpu.VMEM((heads * rows, HEAD), F32),
            pltpu.VMEM((heads * rows, HEAD), F32),
            pltpu.VMEM((heads, CLASSES, class_rows, HEAD), F32),
            pltpu.VMEM((heads, CLASSES, class_rows, HEAD), F32),
            pltpu.VMEM((heads, CLASSES, class_rows, HEAD), F32),
            pltpu.VMEM((heads, CLASSES, class_rows, HEAD), BF16),
            pltpu.VMEM((heads, 8, 128), F32),
            pltpu.VMEM((heads, CLASSES, class_rows, HEAD), BF16),
            pltpu.VMEM((heads, 8, 128), F32),
            pltpu.VMEM((rows, HEAD), F32),
            pltpu.VMEM((rows, 2 * heads * HEAD), BF16),
            pltpu.VMEM((rows, out_cols), F32),
            dma((PIECES,)),
            dma((2, heads)),
            dma((heads // 2,)),
            dma((2, heads)),
            dma((1,)),
            dma((PIECES,)),
            dma((PIECES,)),
            dma((2, heads, 2)),
            dma((2, heads, 2)),
            dma((2, heads)),
            dma((2, heads)),
            dma((2, heads)),
            dma((heads,)),
            dma((heads,)),
        ],
        compiler_params=pltpu.CompilerParams(
            collective_id=0, has_side_effects=True, vmem_limit_bytes=56 * 1024 * 1024
        ),
    )(tokens, query_weight, key_weight, value_weight, output_weight, jnp.asarray(inverse))


def solution(mesh):
    in_specs = (
        P(("grp", "sp", "tp"), None),
        P(None, "tp"),
        P(None, "tp"),
        P(None, "tp"),
        P(None, "tp"),
    )
    out_specs = P(("grp", "sp"), "tp")
    return jax.shard_map(body, mesh=mesh, in_specs=in_specs, out_specs=out_specs, check_vma=False)
```

time: 52.8 us -> 45.6 us (0.86)
  Pallas kernels: 51.7 us -> 44.3 us
    pallas_call x1, Pallas kernels: 51.7 us -> 44.3 us  [body(): pl.pallas_call(functools.partial(kernel, n_sp, heads), out_shape=pltpu.VM...]
where the time goes in v2:
time: 45.6 us; the launch traced here: 45.2 us
  Pallas kernels  44.3 us (97%)
  local copies, waits for them, and re-layouts  0.97 us (2%)
    pallas_call x1, Pallas kernels, body(): pl.pallas_call(functools.partial(kernel, n_sp, heads), out_shape=pltpu.VM...  44.3 us
    unnamed x1, local copies, waits for them, and re-layouts  0.97 us

profile of v2, /device:TPU:11, one launch (start us, length us, event | category | flops | bytes accessed | tf_op | source)
XLA Modules:
  0.0 45.2 jit_solution(15302747305456609969)
XLA Ops:
  0.0 44.3 %shard_map.64 = bf16[512,1024]{1,0:T(8,128)(2,1)S(1)} custom-call(bf16[256,2048]{1,0:T(8,128)(2,1)} %tok_hbm.1, bf16[2048,512]{1,0:T(8,128)(2,1)} %wq_hbm.1, bf16[2048,512]{1,0:T(8,128)(2,1)} %wk_hbm.1, bf16[2048,512]{1,0:T(8,128)(2,1)} %wv_hbm.1, bf16[1024,1024]{1,0:T(8,128)(2,1)} %wo_hbm.1, f32[1,128]{1,0:T(1,128)} %constant.2.clone.inv_hbm), custom_call_target="tpu_custom_call" | custom-call | tf_op jit(solution)/shard_map/pallas_call | solution.py:433
  44.3 1.0 %copy.8 = bf16[512,1024]{1,0:T(8,128)(2,1)} copy(bf16[512,1024]{1,0:T(8,128)(2,1)S(1)} %shard_map.64) | data formatting | bytes 2097152

commit v3 on v2

v3 whole, which is shorter than its diff:
```python
import functools

import jax
import jax.numpy as jnp
import numpy as np
from jax import lax
from jax.experimental import pallas as pl
from jax.experimental.pallas import tpu as pltpu
from jax.sharding import PartitionSpec as P

HEAD = 128
REACH_STEPS = 128
MIDDLE_DILATION = 4
FAR_DILATION = 16
THETA_BASE = 500000.0
NEG = -1e30
MESH = pl.DeviceIdType.MESH
F32 = jnp.float32
BF16 = jnp.bfloat16
SCALE = HEAD ** -0.5 / float(np.log(2.0))

A, C, O = 0, 1, 2
SLOTS = 3
CLASSES = MIDDLE_DILATION
PIECES = 2


def iota(shape, dim):
    return lax.broadcasted_iota(jnp.int32, shape, dim)


def rotated(x, cosine, sine):
    return x * cosine + pltpu.roll(x, HEAD // 2, 1) * sine


def weighed(scores, values):
    top = jnp.max(scores, axis=-1, keepdims=True)
    raised = jnp.exp2(scores - top).astype(BF16)
    ones = jnp.ones(values.shape, BF16)
    both = jnp.dot(raised, jnp.concatenate([values, ones], axis=1), preferred_element_type=F32)
    return both[:, :HEAD], both[:, HEAD:], top


def transposed_dot(a, b):
    return lax.dot_general(a, b, (((1,), (1,)), ((), ())), preferred_element_type=F32)


def classed(start, count, c):
    return pl.ds(start + c, count, stride=CLASSES)


def kernel(
    n_sp, heads, guests,
    tok_hbm, wq_hbm, wk_hbm, wv_hbm, wo_hbm, inv_hbm,
    out_ref,
    x, wkv, wq, wo, inv, cos_ref, sin_ref, ctx, q, qn, kn, vn, visitor, second, flat_a, flat_b,
    far_bias, visit_bias, pair_bias, band, num, tot, top, cnum, ctot, ctop, vnum, vtot, vtop,
    part, part_lse, far_out, far_lse, back, back_lse, mid_out, mid_lse, mixf, mixg, out_sum,
    tok_sem, kv_sem, q_load, wo_sem, inv_sem, x_send, x_recv,
    ctx_send, ctx_recv, q_sem, second_sem, part_sem, lse_sem, mid_sem, mid_lse_sem, mix_send, mix_recv,
):
    sp = lax.axis_index("sp")
    tp = lax.axis_index("tp")
    z = sp // 2
    odd = sp % 2
    even = odd == 0
    other = 1 - tp
    has_next = z + 1 < n_sp // 2
    has_second = z + 2 < n_sp // 2
    half_rows = x.shape[1]
    rows = 2 * half_rows
    class_rows = rows // CLASSES
    half_class = class_rows // 2
    piece = half_rows // PIECES
    order = (tp, other)

    tok_copies = []
    for i in range(PIECES):
        span = pl.ds(i * piece, piece)
        copy = pltpu.make_async_copy(tok_hbm.at[span], x.at[tp, span], tok_sem.at[i])
        copy.start()
        tok_copies.append(copy)
    inv_copy = pltpu.make_async_copy(inv_hbm, inv, inv_sem.at[0])
    inv_copy.start()

    def kv_copy(h, kind):
        source = (wk_hbm, wv_hbm)[kind]
        cols = pl.ds(h * HEAD, HEAD)
        return pltpu.make_async_copy(source.at[:, cols], wkv.at[h, :, pl.ds(kind * HEAD, HEAD)], kv_sem.at[kind, h])

    q_copies = [
        pltpu.make_async_copy(wq_hbm.at[:, pl.ds(p * 2 * HEAD, 2 * HEAD)], wq.at[p], q_load.at[p])
        for p in range(heads // 2)]
    q_copies[0].start()
    for h in (guests, 0):
        for kind in range(2):
            kv_copy(h, kind).start()
    wo_copies = [
        pltpu.make_async_copy(
            wo_hbm.at[pl.ds((t * heads + h) * HEAD, HEAD)], wo.at[pl.ds((2 * h + t) * HEAD, HEAD)], wo_sem.at[t, h])
        for h in range(heads) for t in range(2)]

    barrier = pltpu.get_barrier_semaphore()
    y_partner = sp + 1 - 2 * odd

    def greet(ids):
        pl.semaphore_signal(barrier, inc=1, device_id=ids, device_id_type=MESH)

    greet({"tp": other})
    greet({"sp": y_partner})

    @pl.when(has_next)
    def _():
        greet({"sp": sp + 2})

    @pl.when(z > 0)
    def _():
        greet({"sp": sp - 2})

    def remote(src, dst, send_sem, recv_sem, ids):
        return pltpu.make_async_remote_copy(
            src_ref=src, dst_ref=dst, send_sem=send_sem, recv_sem=recv_sem,
            device_id=ids, device_id_type=MESH)

    down = {"sp": sp + 2}
    up = {"sp": sp - 2}
    side = {"sp": y_partner}
    across = {"tp": other}

    block = REACH_STEPS
    share = block // CLASSES
    ratio = FAR_DILATION // MIDDLE_DILATION

    def masks():
        qi, kj = iota((block, SLOTS * block), 0), iota((block, SLOTS * block), 1)
        slot = kj // block
        apart = qi - (kj % block)

        def bias(dist, here):
            steps = apart + block * dist
            mid = here & (steps >= 0) & (steps <= REACH_STEPS)
            far = here & (steps >= 0) & (steps % ratio == 0) & (steps <= ratio * REACH_STEPS)
            return jnp.where(mid & far, 1.0, jnp.where(mid | far, 0.0, NEG))

        far_bias[...] = bias(O - slot, O - slot <= sp)
        visit_bias[...] = bias(O + 2 - slot, O - slot <= sp)[:, :O * block]
        pair_bias[0] = bias(O - slot, (slot == O) | (odd == 1))[:, C * block:]
        pair_bias[1] = bias(jnp.where(slot == O, 2, 1 + 2 * odd), slot >= C)[:, C * block:]
        pair_bias[2] = bias(jnp.where(slot == O, 4, 3 + 2 * odd), slot >= C)[:, C * block:]
        ni, nj = iota((block, 2 * block), 0), iota((block, 2 * block), 1)
        gap = ni + block - nj
        band[1] = jnp.where((gap >= 0) & (gap <= REACH_STEPS), 0.0, NEG)
        gap = jnp.where(nj < block, ni + block - ((nj % share) * CLASSES + nj // share), gap)
        near_ok = (gap >= 0) & (gap <= REACH_STEPS)
        band[0] = jnp.where(near_ok & ((nj >= block) | (sp > 0)), 0.0, NEG)
        band[2] = jnp.where(near_ok & ((nj >= block) | (odd == 1)), 0.0, NEG)
        gap = ((ni % share) - (nj % share)) * CLASSES + ni // share - nj // share + block
        band[3] = jnp.where((gap >= 0) & (gap <= REACH_STEPS) & even & (nj < block), 0.0, NEG)

        for slot_at in (A, C):
            @pl.when(sp < 2 - slot_at)
            def _():
                def clear(h, _):
                    ctx[h, :, :, slot_at] = jnp.zeros((2, CLASSES, class_rows, HEAD), BF16)
                    return 0
                lax.fori_loop(guests, heads, clear, 0)

        part_lse[...] = jnp.zeros(part_lse.shape, F32)
        back_lse[...] = jnp.zeros(back_lse.shape, F32)

        @pl.when(z == 0)
        def _():
            far_out[...] = jnp.zeros(far_out.shape, BF16)
            far_lse[...] = jnp.full(far_lse.shape, NEG, F32)
            mid_out[...] = jnp.zeros(mid_out.shape, BF16)
            mid_lse[...] = jnp.full(mid_lse.shape, NEG, F32)

    lane = iota((piece, HEAD), 1)

    def table(c, _):
        start = pl.multiple_of(c * piece, piece)
        positions = sp * rows + start + iota((piece, HEAD), 0)
        angles = positions.astype(F32) * inv[...]
        span = pl.ds(start, piece)
        cos_ref[span, :] = jnp.cos(angles)
        sine = jnp.sin(angles)
        sin_ref[span, :] = jnp.where(lane < HEAD // 2, -sine, sine)
        return 0

    inv_copy.wait()
    lax.fori_loop(tp * PIECES, tp * PIECES + PIECES, table, 0)

    pl.semaphore_wait(barrier, 2 + has_next.astype(jnp.int32) + (z > 0).astype(jnp.int32))

    def x_copy(i):
        span = pl.ds(i * piece, piece)
        return remote(x.at[tp, span], x.at[tp, span], x_send.at[i], x_recv.at[i], across)

    for i in range(PIECES):
        tok_copies[i].wait()
        x_copy(i).start()
    for h in (*range(1, guests), *range(guests + 1, heads)):
        for kind in range(2):
            kv_copy(h, kind).start()
    for copy in (*q_copies[1:], *wo_copies):
        copy.start()

    def send(h, half, src, dst, ids):
        spots = pl.ds(pl.multiple_of(half * half_class, half_class), half_class)
        return remote(ctx.at[h, :, :, src, spots], ctx.at[h, :, :, dst, spots],
                      ctx_send.at[dst, h, half], ctx_recv.at[dst, h, half], ids)

    def send_down(h, half):
        return () if h < guests else ((has_next, send(h, half, O, A, down)),)

    def send_side(h, half):
        return ((even | (h < guests), send(h, half, O, C, side)),)

    def send_relay(h, half):
        return () if h < guests else (((odd == 1) & (z > 0), send(h, half, A, C, side)),)

    def query_copy(h, half):
        spots = pl.ds(pl.multiple_of(half * half_class, half_class), half_class)
        return remote(q.at[h, :, spots], visitor.at[h, :, spots], q_sem.at[0, h, half], q_sem.at[1, h, half], up)

    def send_query(h, half):
        return ((z > 0, query_copy(h, half)),)

    def second_copy(h):
        return remote(visitor.at[h], second.at[h], second_sem.at[0, h], second_sem.at[1, h], up)

    def send_second(h):
        return ((has_next & (z > 0), second_copy(h)),) if h < guests else ()

    def back_copies(h):
        return (remote(back.at[h], mid_out.at[h], mid_sem.at[0, h], mid_sem.at[1, h], down),
                remote(back_lse.at[h], mid_lse.at[h], mid_lse_sem.at[0, h], mid_lse_sem.at[1, h], down))

    def send_back(h):
        return tuple((has_second, copy) for copy in back_copies(h)) if h < guests else ()

    def send_part(h):
        return ((has_next, remote(part.at[h], far_out.at[h], part_sem.at[0, h], part_sem.at[1, h], down)),
                (has_next, remote(part_lse.at[h], far_lse.at[h], lse_sem.at[0, h], lse_sem.at[1, h], down)))

    def start_all(sends):
        for condition, copy in sends:
            @pl.when(condition)
            def _():
                copy.start()

    def project_kv(h, half):
        if half is None:
            source, natural, span = x[...].reshape(rows, x.shape[2]), pl.ds(0, rows), (0, rows)
            spots = pl.ds(0, class_rows)
        else:
            source, natural = x[half], pl.ds(pl.multiple_of(half * half_rows, half_rows), half_rows)
            span, spots = (0, half_rows), pl.ds(pl.multiple_of(half * half_class, half_class), half_class)
        kv = jnp.dot(source, wkv[h], preferred_element_type=F32)
        k = rotated(kv[:, :HEAD], cos_ref[natural], sin_ref[natural])
        v = kv[:, HEAD:]
        flat_a[span[0]:span[1]] = k
        flat_b[span[0]:span[1]] = v
        kn[h, natural] = k.astype(BF16)
        vn[h, natural] = v.astype(BF16)
        count = span[1] // CLASSES
        for c in range(CLASSES):
            ctx[h, 0, c, O, spots] = flat_a[classed(0, count, c), :].astype(BF16)
            ctx[h, 1, c, O, spots] = flat_b[classed(0, count, c), :].astype(BF16)
        for part_half in (order if half is None else (half,)):
            start_all(send_down(h, part_half))
            if h < guests:
                start_all(send_side(h, part_half))

    def project_q(p, half):
        if half is None:
            source, natural, count = x[...].reshape(rows, x.shape[2]), pl.ds(0, rows), rows
            spots = pl.ds(0, class_rows)
        else:
            source, natural = x[half], pl.ds(pl.multiple_of(half * half_rows, half_rows), half_rows)
            count, spots = half_rows, pl.ds(pl.multiple_of(half * half_class, half_class), half_class)
        qq = jnp.dot(source, wq[p], preferred_element_type=F32)
        for s, flat in ((0, flat_a), (1, flat_b)):
            r = rotated(qq[:, s * HEAD:(s + 1) * HEAD], cos_ref[natural], sin_ref[natural])
            flat[0:count] = r
            qn[2 * p + s, natural] = r.astype(BF16)
            for c in range(CLASSES):
                q[2 * p + s, c, spots] = flat[classed(0, count // CLASSES, c), :].astype(BF16)
            if half is not None:
                start_all(send_query(2 * p + s, half))

    def load_kv(h):
        kv_copy(h, 0).wait()
        kv_copy(h, 1).wait()

    def near(h, b, keys, vals, bias):
        scores = transposed_dot(qn[h, b * block:(b + 1) * block], keys) * SCALE + bias
        n, t, m = weighed(scores, vals)
        span = pl.ds(pl.multiple_of(h * rows, rows) + b * block, block)
        num[span, :] = n
        tot[span, :] = t
        top[span, :] = jnp.broadcast_to(m, (block, HEAD))

    def near_inner(h, _):
        for b in range(1, rows // block):
            span = slice((b - 1) * block, (b + 1) * block)
            near(h, b, kn[h, span], vn[h, span], band[1])
        return 0

    def load_kv(h):
        kv_copy(h, 0).wait()
        kv_copy(h, 1).wait()

    def poll(h):
        for half in order:
            @pl.when((odd == 1) & (z > 0))
            def _():
                send(h, half, A, A, side).wait_recv()
            start_all(send_relay(h, half))

    def meet(h):
        @pl.when(has_next)
        def _():
            for half in order:
                query_copy(h, half).wait_recv()
        start_all(send_second(h))

    def neighbours(h):
        for half in order:
            if h >= guests:
                @pl.when(even & (z > 0))
                def _():
                    send(h, half, A, A, side).wait_recv()

                @pl.when(sp > 0)
                def _():
                    send(h, half, C, C, side).wait_recv()
            else:
                send(h, half, C, C, side).wait_recv()

    def mix_copy(h):
        cols = pl.ds(pl.multiple_of((2 * h + tp) * HEAD, HEAD), HEAD)
        return remote(mixg.at[:, cols], mixg.at[:, cols], mix_send.at[h], mix_recv.at[h], across)

    eye = iota((block, block), 0) == iota((block, block), 1)

    def context(h, c, kind, first, last):
        return ctx[h, kind, c, first:last].reshape((last - first) * class_rows, HEAD)

    def visit(h, guest, bias, first, last, result, lse):
        for c in range(CLASSES):
            keys, vals = (context(h, c, kind, first, last) for kind in range(2))
            n, t, m = weighed(transposed_dot(guest[h, c], keys) * SCALE + bias, vals)
            result[h, c] = (n / t).astype(BF16)
            lse[h, c:c + 1, :] = jnp.sum(jnp.where(eye, m + jnp.log2(t), 0.0), axis=0, keepdims=True)

    def visit_far(h):
        meet(h)

        @pl.when(has_next)
        def _():
            visit(h, visitor, visit_bias[...], A, O, part, part_lse)
        start_all(send_part(h))

    def visit_second(h):
        @pl.when(has_second)
        def _():
            second_copy(h).wait_recv()
            visit(h, second, pair_bias[2], C, SLOTS, back, back_lse)
        start_all(send_back(h))

    def tail_of(h, kind):
        return [ctx[h, kind, c, C, class_rows - share:] for c in range(CLASSES)]

    def join(n, t, m, n2, t2, m2):
        most = jnp.maximum(m, m2)
        old, new = jnp.exp2(m - most), jnp.exp2(m2 - most)
        return n * old + n2 * new, t * old + t2 * new, most

    def visit_first(h):
        @pl.when(has_next)
        def _():
            keys, vals = (jnp.concatenate(tail_of(h, kind), axis=0) for kind in range(2))
            guest = jnp.concatenate([visitor[h, c, :share] for c in range(CLASSES)], axis=0)
            close = weighed(transposed_dot(guest, keys) * SCALE + band[3, :, :block], vals)
            for c in range(CLASSES):
                keys, vals = (context(h, c, kind, C, SLOTS) for kind in range(2))
                n, t, m = weighed(transposed_dot(visitor[h, c], keys) * SCALE + pair_bias[1], vals)
                m = jnp.broadcast_to(m, (block, HEAD))
                vnum[h, c], vtot[h, c], vtop[h, c] = n, t, m
                n, t, m = join(n[:share], t[:share], m[:share], *(v[c * share:(c + 1) * share] for v in close))
                vnum[h, c, :share], vtot[h, c, :share], vtop[h, c, :share] = n, t, m

    def with_far(n, t, m, result, lse_row):
        lf = jnp.sum(jnp.where(eye, lse_row, 0.0), axis=1, keepdims=True)
        most = jnp.maximum(m, lf)
        en, ef = jnp.exp2(m - most), jnp.exp2(lf - most)
        total = t * en + ef
        return (n * en + result.astype(F32) * ef) / total, total, most

    def merge(h):
        @pl.when(has_next)
        def _():
            @pl.when(z > 0)
            def _():
                for copy in back_copies(h):
                    copy.wait_recv()
            for c in range(CLASSES):
                r, t, m = with_far(vnum[h, c], vtot[h, c], vtop[h, c], mid_out[h, c], mid_lse[h, c:c + 1, :])
                part[h, c] = r.astype(BF16)
                part_lse[h, c:c + 1, :] = jnp.sum(jnp.where(eye, m + jnp.log2(t), 0.0), axis=0, keepdims=True)
        start_all(send_part(h))

    def attend(h):
        first, bias, close = (C, pair_bias[0], band[2]) if h < guests else (A, far_bias[...], band[0])
        keys, vals = (jnp.concatenate(tail_of(h, kind) + [nat[h, :block]], axis=0)
                      for kind, nat in ((0, kn), (1, vn)))
        near(h, 0, keys, vals, close)
        for c in range(CLASSES):
            keys, vals = (context(h, c, kind, first, SLOTS) for kind in range(2))
            n, t, m = weighed(transposed_dot(q[h, c], keys) * SCALE + bias, vals)
            span = classed(h * rows, class_rows, c)
            cnum[h, c], ctot[h, c], ctop[h, c] = join(num[span, :], tot[span, :], top[span, :], n, t, m)

    def combine(h, _):
        @pl.when(z > 0)
        def _():
            remote(part.at[h], far_out.at[h], part_sem.at[0, h], part_sem.at[1, h], side).wait_recv()
            remote(part_lse.at[h], far_lse.at[h], lse_sem.at[0, h], lse_sem.at[1, h], side).wait_recv()

        for c in range(CLASSES):
            mixed, _, _ = with_far(cnum[h, c], ctot[h, c], ctop[h, c], far_out[h, c], far_lse[h, pl.ds(c, 1), :])
            mixf[classed(0, class_rows, c), :] = mixed
        cols = pl.ds(pl.multiple_of((2 * h + tp) * HEAD, HEAD), HEAD)
        mixg[:, cols] = mixf[...].astype(BF16)
        mix_copy(h).start()
        return 0

    def gathered(h, _):
        mix_copy(h).wait_recv()
        return 0

    out_cols = out_ref.shape[1]
    wide = 256

    def add_last(t, into):
        span = pl.ds(pl.multiple_of((2 * (heads - 1) + t) * HEAD, HEAD), HEAD)
        for i in range(out_cols // wide):
            cols = pl.ds(i * wide, wide)
            total = jnp.dot(mixg[:, span], wo[span, cols], preferred_element_type=F32)
            into[:, cols] = (out_sum[:, cols] + total).astype(into.dtype)

    def partial_out():
        most_in = (heads - 1) * 2 * HEAD
        for i in range(out_cols // wide):
            cols = pl.ds(i * wide, wide)
            out_sum[:, cols] = jnp.dot(mixg[:, :most_in], wo[:most_in, cols], preferred_element_type=F32)

    q_copies[0].wait()
    project_q(0, tp)
    load_kv(guests)
    project_kv(guests, tp)
    load_kv(0)
    project_kv(0, tp)
    lax.fori_loop(other * PIECES, other * PIECES + PIECES, table, 0)
    for i in range(PIECES):
        x_copy(i).wait_recv()
    project_q(0, other)
    project_kv(guests, other)
    project_kv(0, other)
    for h in (*range(1, guests), *range(guests + 1, heads)):
        load_kv(h)
        project_kv(h, None)
    for h in range(guests, heads):
        for half in order:
            start_all(send_side(h, half))
    meet(0)
    for p in range(1, heads // 2):
        q_copies[p].wait()
        project_q(p, None)
    masks()
    for h in range(1, guests):
        meet(h)
    for h in range(2, heads):
        for half in order:
            start_all(send_query(h, half))
    lax.fori_loop(0, heads // 2, near_inner, 0)
    poll(guests)
    lax.fori_loop(heads // 2, heads, near_inner, 0)
    neighbours(0)
    visit_first(0)
    attend(0)
    visit_second(0)
    for h in range(1, guests):
        poll(guests + h)
        neighbours(h)
        visit_second(h)
        visit_first(h)
        attend(h)
    for h in range(2 * guests, heads):
        poll(h)
    for h in range(guests):
        merge(h)
    for h in range(guests, heads):
        neighbours(h)
        visit_far(h)
        attend(h)
        if h < heads - 1:
            combine(h - guests, 0)
    for h in range(heads - guests - 1, heads - 1):
        combine(h, 0)
    for copy in wo_copies:
        copy.wait()
    for h in range(heads - 1):
        gathered(h, 0)
    partial_out()
    combine(heads - 1, 0)
    add_last(tp, out_sum)
    gathered(heads - 1, 0)
    add_last(other, out_ref)

    for i in range(PIECES):
        x_copy(i).wait_send()

    for h in range(heads):
        sends = send_second(h) + send_back(h) + send_part(h)
        for half in range(2):
            sends = sends + send_down(h, half) + send_side(h, half) + send_relay(h, half) + send_query(h, half)
        for condition, copy in sends:
            @pl.when(condition)
            def _():
                copy.wait_send()
        mix_copy(h).wait_send()


def body(tokens, query_weight, key_weight, value_weight, output_weight):
    n_sp = lax.axis_size("sp")
    half_rows, width = tokens.shape
    rows = half_rows * lax.axis_size("tp")
    heads = query_weight.shape[1] // HEAD
    assert rows * 4 == FAR_DILATION * REACH_STEPS and rows == 512
    assert n_sp % 2 == 0 and lax.axis_size("tp") == 2 and heads % 2 == 0 and heads >= 4

    half = HEAD // 2
    inverse = THETA_BASE ** (-np.arange(half, dtype=np.float64) / half)
    inverse = np.concatenate([inverse, inverse]).astype(np.float32)[None, :]

    guests = heads // 2
    class_rows = rows // CLASSES
    anywhere = pl.BlockSpec(memory_space=pl.ANY)
    vmem = pl.BlockSpec(memory_space=pltpu.VMEM)
    out_cols = output_weight.shape[1]
    dma = pltpu.SemaphoreType.DMA
    return pl.pallas_call(
        functools.partial(kernel, n_sp, heads, guests),
        out_shape=pltpu.VMEM((rows, out_cols), BF16),
        in_specs=[anywhere] * 6,
        out_specs=vmem,
        scratch_shapes=[
            pltpu.VMEM((2, half_rows, width), BF16),
            pltpu.VMEM((heads, width, 2 * HEAD), BF16),
            pltpu.VMEM((heads // 2, width, 2 * HEAD), BF16),
            pltpu.VMEM(output_weight.shape, BF16),
            pltpu.VMEM((1, HEAD), F32),
            pltpu.VMEM((rows, HEAD), F32),
            pltpu.VMEM((rows, HEAD), F32),
            pltpu.VMEM((heads, 2, CLASSES, SLOTS, class_rows, HEAD), BF16),
            pltpu.VMEM((heads, CLASSES, class_rows, HEAD), BF16),
            pltpu.VMEM((heads, rows, HEAD), BF16),
            pltpu.VMEM((heads, rows, HEAD), BF16),
            pltpu.VMEM((heads, rows, HEAD), BF16),
            pltpu.VMEM((heads, CLASSES, class_rows, HEAD), BF16),
            pltpu.VMEM((guests, CLASSES, class_rows, HEAD), BF16),
            pltpu.VMEM((rows, HEAD), F32),
            pltpu.VMEM((rows, HEAD), F32),
            pltpu.VMEM((REACH_STEPS, SLOTS * REACH_STEPS), F32),
            pltpu.VMEM((REACH_STEPS, 2 * REACH_STEPS), F32),
            pltpu.VMEM((3, REACH_STEPS, 2 * REACH_STEPS), F32),
            pltpu.VMEM((4, REACH_STEPS, 2 * REACH_STEPS), F32),
            pltpu.VMEM((heads * rows, HEAD), F32),
            pltpu.VMEM((heads * rows, HEAD), F32),
            pltpu.VMEM((heads * rows, HEAD), F32),
            pltpu.VMEM((heads, CLASSES, class_rows, HEAD), F32),
            pltpu.VMEM((heads, CLASSES, class_rows, HEAD), F32),
            pltpu.VMEM((heads, CLASSES, class_rows, HEAD), F32),
            pltpu.VMEM((guests, CLASSES, class_rows, HEAD), F32),
            pltpu.VMEM((guests, CLASSES, class_rows, HEAD), F32),
            pltpu.VMEM((guests, CLASSES, class_rows, HEAD), F32),
            pltpu.VMEM((heads, CLASSES, class_rows, HEAD), BF16),
            pltpu.VMEM((heads, 8, 128), F32),
            pltpu.VMEM((heads, CLASSES, class_rows, HEAD), BF16),
            pltpu.VMEM((heads, 8, 128), F32),
            pltpu.VMEM((guests, CLASSES, class_rows, HEAD), BF16),
            pltpu.VMEM((guests, 8, 128), F32),
            pltpu.VMEM((guests, CLASSES, class_rows, HEAD), BF16),
            pltpu.VMEM((guests, 8, 128), F32),
            pltpu.VMEM((rows, HEAD), F32),
            pltpu.VMEM((rows, 2 * heads * HEAD), BF16),
            pltpu.VMEM((rows, out_cols), F32),
            dma((PIECES,)),
            dma((2, heads)),
            dma((heads // 2,)),
            dma((2, heads)),
            dma((1,)),
            dma((PIECES,)),
            dma((PIECES,)),
            dma((2, heads, 2)),
            dma((2, heads, 2)),
            dma((2, heads, 2)),
            dma((2, guests)),
            dma((2, heads)),
            dma((2, heads)),
            dma((2, guests)),
            dma((2, guests)),
            dma((heads,)),
            dma((heads,)),
        ],
        compiler_params=pltpu.CompilerParams(
            collective_id=0, has_side_effects=True, vmem_limit_bytes=56 * 1024 * 1024
        ),
    )(tokens, query_weight, key_weight, value_weight, output_weight, jnp.asarray(inverse))


def solution(mesh):
    in_specs = (
        P(("grp", "sp", "tp"), None),
        P(None, "tp"),
        P(None, "tp"),
        P(None, "tp"),
        P(None, "tp"),
    )
    out_specs = P(("grp", "sp"), "tp")
    return jax.shard_map(body, mesh=mesh, in_specs=in_specs, out_specs=out_specs, check_vma=False)
```

time: 45.6 us -> 38.6 us (0.85)
  Pallas kernels: 44.3 us -> 37.3 us
    pallas_call x1, Pallas kernels: 44.3 us -> 37.3 us  [body(): pl.pallas_call(functools.partial(kernel, n_sp, heads, guests), out_shape=...]
where the time goes in v3:
time: 38.6 us; the launch traced here: 38.3 us
  Pallas kernels  37.3 us (97%)
  local copies, waits for them, and re-layouts  0.97 us (3%)
    pallas_call x1, Pallas kernels, body(): pl.pallas_call(functools.partial(kernel, n_sp, heads, guests), out_shape=...  37.3 us
    unnamed x1, local copies, waits for them, and re-layouts  0.97 us

profile of v3, /device:TPU:11, one launch (start us, length us, event | category | flops | bytes accessed | tf_op | source)
XLA Modules:
  0.0 38.3 jit_solution(7366455605610177891)
XLA Ops:
  0.0 37.3 %shard_map.64 = bf16[512,1024]{1,0:T(8,128)(2,1)S(1)} custom-call(bf16[256,2048]{1,0:T(8,128)(2,1)} %tok_hbm.1, bf16[2048,512]{1,0:T(8,128)(2,1)} %wq_hbm.1, bf16[2048,512]{1,0:T(8,128)(2,1)} %wk_hbm.1, bf16[2048,512]{1,0:T(8,128)(2,1)} %wv_hbm.1, bf16[1024,1024]{1,0:T(8,128)(2,1)} %wo_hbm.1, f32[1,128]{1,0:T(1,128)} %constant.2.clone.inv_hbm), custom_call_target="tpu_custom_call" | custom-call | tf_op jit(solution)/shard_map/pallas_call | solution.py:554
  37.4 1.0 %copy.8 = bf16[512,1024]{1,0:T(8,128)(2,1)} copy(bf16[512,1024]{1,0:T(8,128)(2,1)S(1)} %shard_map.64) | data formatting | bytes 2097152

commit v4 on v3

--- a/solution.py
+++ b/solution.py
@@ -56,8 +56,8 @@
     x, wkv, wq, wo, inv, cos_ref, sin_ref, ctx, q, qn, kn, vn, visitor, second, flat_a, flat_b,
     far_bias, visit_bias, pair_bias, band, num, tot, top, cnum, ctot, ctop, vnum, vtot, vtop,
     part, part_lse, far_out, far_lse, back, back_lse, mid_out, mid_lse, mixf, mixg, out_sum,
-    tok_sem, kv_sem, q_load, wo_sem, inv_sem, x_send, x_recv,
-    ctx_send, ctx_recv, q_sem, second_sem, part_sem, lse_sem, mid_sem, mid_lse_sem, mix_send, mix_recv,
+    tok_sem, inv_sem, kv_sem, q_load, wo_sem, x_sem, sent,
+    a_recv, c_recv, q_recv, second_recv, part_recv, lse_recv, mid_recv, mid_lse_recv, mix_recv,
 ):
     sp = lax.axis_index("sp")
     tp = lax.axis_index("tp")
@@ -74,30 +74,24 @@
     piece = half_rows // PIECES
     order = (tp, other)
 
-    tok_copies = []
-    for i in range(PIECES):
-        span = pl.ds(i * piece, piece)
-        copy = pltpu.make_async_copy(tok_hbm.at[span], x.at[tp, span], tok_sem.at[i])
-        copy.start()
-        tok_copies.append(copy)
     inv_copy = pltpu.make_async_copy(inv_hbm, inv, inv_sem.at[0])
     inv_copy.start()
+    tok_copy = pltpu.make_async_copy(tok_hbm, x.at[tp], tok_sem.at[0])
+    tok_copy.start()
 
     def kv_copy(h, kind):
         source = (wk_hbm, wv_hbm)[kind]
         cols = pl.ds(h * HEAD, HEAD)
-        return pltpu.make_async_copy(source.at[:, cols], wkv.at[h, :, pl.ds(kind * HEAD, HEAD)], kv_sem.at[kind, h])
+        return pltpu.make_async_copy(source.at[:, cols], wkv.at[h, :, pl.ds(kind * HEAD, HEAD)], kv_sem.at[h])
 
     q_copies = [
         pltpu.make_async_copy(wq_hbm.at[:, pl.ds(p * 2 * HEAD, 2 * HEAD)], wq.at[p], q_load.at[p])
         for p in range(heads // 2)]
-    q_copies[0].start()
-    for h in (guests, 0):
-        for kind in range(2):
-            kv_copy(h, kind).start()
+    for kind in range(2):
+        kv_copy(guests, kind).start()
     wo_copies = [
         pltpu.make_async_copy(
-            wo_hbm.at[pl.ds((t * heads + h) * HEAD, HEAD)], wo.at[pl.ds((2 * h + t) * HEAD, HEAD)], wo_sem.at[t, h])
+            wo_hbm.at[pl.ds((t * heads + h) * HEAD, HEAD)], wo.at[pl.ds((2 * h + t) * HEAD, HEAD)], wo_sem.at[0])
         for h in range(heads) for t in range(2)]
 
     barrier = pltpu.get_barrier_semaphore()
@@ -188,60 +182,62 @@
         return 0
 
     inv_copy.wait()
+    for kind in range(2):
+        kv_copy(0, kind).start()
+    q_copies[0].start()
     lax.fori_loop(tp * PIECES, tp * PIECES + PIECES, table, 0)
 
     pl.semaphore_wait(barrier, 2 + has_next.astype(jnp.int32) + (z > 0).astype(jnp.int32))
 
-    def x_copy(i):
-        span = pl.ds(i * piece, piece)
-        return remote(x.at[tp, span], x.at[tp, span], x_send.at[i], x_recv.at[i], across)
-
-    for i in range(PIECES):
-        tok_copies[i].wait()
-        x_copy(i).start()
-    for h in (*range(1, guests), *range(guests + 1, heads)):
+    x_copy = remote(x.at[tp], x.at[tp], x_sem.at[0], x_sem.at[1], across)
+    tok_copy.wait()
+    x_copy.start()
+    for h in (*range(guests + 1, heads), *range(1, guests)):
         for kind in range(2):
             kv_copy(h, kind).start()
     for copy in (*q_copies[1:], *wo_copies):
         copy.start()
 
-    def send(h, half, src, dst, ids):
-        spots = pl.ds(pl.multiple_of(half * half_class, half_class), half_class)
-        return remote(ctx.at[h, :, :, src, spots], ctx.at[h, :, :, dst, spots],
-                      ctx_send.at[dst, h, half], ctx_recv.at[dst, h, half], ids)
+    DOWN, SIDE, RELAY, ASK, SECOND, PART, LSE, MID, MID_LSE, MIX = range(10)
+
+    def spots_of(half):
+        return pl.ds(pl.multiple_of(half * half_class, half_class), half_class)
+
+    def block_copy(h, src, dst, rows_at, kind, ids):
+        arrived = a_recv.at[h - guests] if dst == A else c_recv.at[h]
+        return remote(ctx.at[h, :, :, src, rows_at], ctx.at[h, :, :, dst, rows_at], sent.at[kind], arrived, ids)
+
+    every = pl.ds(0, class_rows)
 
     def send_down(h, half):
-        return () if h < guests else ((has_next, send(h, half, O, A, down)),)
+        return ((has_next & (h >= guests), block_copy(jnp.maximum(h, guests), O, A, spots_of(half), DOWN, down)),)
 
     def send_side(h, half):
-        return ((even | (h < guests), send(h, half, O, C, side)),)
-
-    def send_relay(h, half):
-        return () if h < guests else (((odd == 1) & (z > 0), send(h, half, A, C, side)),)
+        return ((even | (h < guests), block_copy(h, O, C, spots_of(half), SIDE, side)),)
+
+    def send_relay(h):
+        return (((odd == 1) & (z > 0), block_copy(h, A, C, every, RELAY, side)),)
 
     def query_copy(h, half):
-        spots = pl.ds(pl.multiple_of(half * half_class, half_class), half_class)
-        return remote(q.at[h, :, spots], visitor.at[h, :, spots], q_sem.at[0, h, half], q_sem.at[1, h, half], up)
-
-    def send_query(h, half):
-        return ((z > 0, query_copy(h, half)),)
-
-    def second_copy(h):
-        return remote(visitor.at[h], second.at[h], second_sem.at[0, h], second_sem.at[1, h], up)
-
-    def send_second(h):
-        return ((has_next & (z > 0), second_copy(h)),) if h < guests else ()
+        rows_at, arrived = (spots_of(half), q_recv.at[2 * h + half]) if h < guests else (every, q_recv.at[guests + h])
+        return remote(q.at[h, :, rows_at], visitor.at[h, :, rows_at], sent.at[ASK], arrived, up)
+
+    def second_copy(h, rows_at):
+        return remote(visitor.at[h, :, rows_at], second.at[h, :, rows_at], sent.at[SECOND], second_recv.at[h], up)
 
     def back_copies(h):
-        return (remote(back.at[h], mid_out.at[h], mid_sem.at[0, h], mid_sem.at[1, h], down),
-                remote(back_lse.at[h], mid_lse.at[h], mid_lse_sem.at[0, h], mid_lse_sem.at[1, h], down))
+        return (remote(back.at[h], mid_out.at[h], sent.at[MID], mid_recv.at[h], down),
+                remote(back_lse.at[h], mid_lse.at[h], sent.at[MID_LSE], mid_lse_recv.at[h], down))
+
+    def part_copies(h):
+        return (remote(part.at[h], far_out.at[h], sent.at[PART], part_recv.at[h], down),
+                remote(part_lse.at[h], far_lse.at[h], sent.at[LSE], lse_recv.at[h], down))
 
     def send_back(h):
-        return tuple((has_second, copy) for copy in back_copies(h)) if h < guests else ()
+        return tuple((has_second, copy) for copy in back_copies(h))
 
     def send_part(h):
-        return ((has_next, remote(part.at[h], far_out.at[h], part_sem.at[0, h], part_sem.at[1, h], down)),
-                (has_next, remote(part_lse.at[h], far_lse.at[h], lse_sem.at[0, h], lse_sem.at[1, h], down)))
+        return tuple((has_next, copy) for copy in part_copies(h))
 
     def start_all(sends):
         for condition, copy in sends:
@@ -269,8 +265,10 @@
             ctx[h, 1, c, O, spots] = flat_b[classed(0, count, c), :].astype(BF16)
         for part_half in (order if half is None else (half,)):
             start_all(send_down(h, part_half))
-            if h < guests:
-                start_all(send_side(h, part_half))
+            for condition, copy in send_side(h, part_half):
+                @pl.when(h < guests)
+                def _():
+                    copy.start()
 
     def project_q(p, half):
         if half is None:
@@ -286,12 +284,6 @@
             qn[2 * p + s, natural] = r.astype(BF16)
             for c in range(CLASSES):
                 q[2 * p + s, c, spots] = flat[classed(0, count // CLASSES, c), :].astype(BF16)
-            if half is not None:
-                start_all(send_query(2 * p + s, half))
-
-    def load_kv(h):
-        kv_copy(h, 0).wait()
-        kv_copy(h, 1).wait()
 
     def near(h, b, keys, vals, bias):
         scores = transposed_dot(qn[h, b * block:(b + 1) * block], keys) * SCALE + bias
@@ -301,46 +293,44 @@
         tot[span, :] = t
         top[span, :] = jnp.broadcast_to(m, (block, HEAD))
 
-    def near_inner(h, _):
+    def near_inner(h):
         for b in range(1, rows // block):
             span = slice((b - 1) * block, (b + 1) * block)
             near(h, b, kn[h, span], vn[h, span], band[1])
-        return 0
 
     def load_kv(h):
-        kv_copy(h, 0).wait()
-        kv_copy(h, 1).wait()
+        pltpu.make_async_copy(wk_hbm.at[:, pl.ds(0, 2 * HEAD)], wkv.at[h], kv_sem.at[h]).wait()
 
     def poll(h):
-        for half in order:
-            @pl.when((odd == 1) & (z > 0))
+        @pl.when((odd == 1) & (z > 0))
+        def _():
+            block_copy(h, A, A, every, RELAY, side).wait_recv()
+        start_all(send_relay(h))
+
+    def meet(h, half):
+        @pl.when(has_next)
+        def _():
+            query_copy(h, half).wait_recv()
+        if h < guests:
+            @pl.when(has_next & (z > 0))
             def _():
-                send(h, half, A, A, side).wait_recv()
-            start_all(send_relay(h, half))
-
-    def meet(h):
-        @pl.when(has_next)
-        def _():
-            for half in order:
-                query_copy(h, half).wait_recv()
-        start_all(send_second(h))
+                second_copy(h, spots_of(half)).start()
 
     def neighbours(h):
-        for half in order:
-            if h >= guests:
-                @pl.when(even & (z > 0))
-                def _():
-                    send(h, half, A, A, side).wait_recv()
-
-                @pl.when(sp > 0)
-                def _():
-                    send(h, half, C, C, side).wait_recv()
-            else:
-                send(h, half, C, C, side).wait_recv()
+        if h < guests:
+            block_copy(h, C, C, every, SIDE, side).wait_recv()
+        else:
+            @pl.when(even & (z > 0))
+            def _():
+                block_copy(h, A, A, every, RELAY, side).wait_recv()
+
+            @pl.when(sp > 0)
+            def _():
+                block_copy(h, C, C, every, SIDE, side).wait_recv()
 
     def mix_copy(h):
         cols = pl.ds(pl.multiple_of((2 * h + tp) * HEAD, HEAD), HEAD)
-        return remote(mixg.at[:, cols], mixg.at[:, cols], mix_send.at[h], mix_recv.at[h], across)
+        return remote(mixg.at[:, cols], mixg.at[:, cols], sent.at[MIX], mix_recv.at[h], across)
 
     eye = iota((block, block), 0) == iota((block, block), 1)
 
@@ -355,7 +345,7 @@
             lse[h, c:c + 1, :] = jnp.sum(jnp.where(eye, m + jnp.log2(t), 0.0), axis=0, keepdims=True)
 
     def visit_far(h):
-        meet(h)
+        meet(h, 0)
 
         @pl.when(has_next)
         def _():
@@ -365,7 +355,7 @@
     def visit_second(h):
         @pl.when(has_second)
         def _():
-            second_copy(h).wait_recv()
+            second_copy(h, every).wait_recv()
             visit(h, second, pair_bias[2], C, SLOTS, back, back_lse)
         start_all(send_back(h))
 
@@ -425,8 +415,8 @@
     def combine(h, _):
         @pl.when(z > 0)
         def _():
-            remote(part.at[h], far_out.at[h], part_sem.at[0, h], part_sem.at[1, h], side).wait_recv()
-            remote(part_lse.at[h], far_lse.at[h], lse_sem.at[0, h], lse_sem.at[1, h], side).wait_recv()
+            for copy in part_copies(h):
+                copy.wait_recv()
 
         for c in range(CLASSES):
             mixed, _, _ = with_far(cnum[h, c], ctot[h, c], ctop[h, c], far_out[h, c], far_lse[h, pl.ds(c, 1), :])
@@ -456,49 +446,71 @@
             cols = pl.ds(i * wide, wide)
             out_sum[:, cols] = jnp.dot(mixg[:, :most_in], wo[:most_in, cols], preferred_element_type=F32)
 
+    def ask(h, half):
+        @pl.when(z > 0)
+        def _():
+            query_copy(h, half).start()
+
+    load_kv(guests)
+    project_kv(guests, tp)
     q_copies[0].wait()
     project_q(0, tp)
-    load_kv(guests)
-    project_kv(guests, tp)
+    for h in range(guests):
+        ask(h, tp)
     load_kv(0)
     project_kv(0, tp)
     lax.fori_loop(other * PIECES, other * PIECES + PIECES, table, 0)
-    for i in range(PIECES):
-        x_copy(i).wait_recv()
+    x_copy.wait_recv()
+    project_kv(guests, other)
     project_q(0, other)
-    project_kv(guests, other)
+    ask(0, other)
     project_kv(0, other)
-    for h in (*range(1, guests), *range(guests + 1, heads)):
+
+    def project_rest(i, _):
+        late = heads - guests - 1
+        h = jnp.where(i < late, guests + 1 + i, i - late + 1)
         load_kv(h)
         project_kv(h, None)
+        for g in range(1, guests):
+            @pl.when(i == g - 1)
+            def _():
+                ask(g, other)
+        return 0
+
+    lax.fori_loop(0, heads - 2, project_rest, 0)
     for h in range(guests, heads):
         for half in order:
             start_all(send_side(h, half))
-    meet(0)
+    meet(0, tp)
+    masks()
+    meet(0, other)
+    for h in range(1, guests):
+        meet(h, tp)
+    near_inner(0)
+    near_inner(1)
+    neighbours(0)
+    visit_first(0)
+    for h in range(1, guests):
+        meet(h, other)
+    poll(guests)
+    attend(0)
     for p in range(1, heads // 2):
         q_copies[p].wait()
         project_q(p, None)
-    masks()
-    for h in range(1, guests):
-        meet(h)
-    for h in range(2, heads):
-        for half in order:
-            start_all(send_query(h, half))
-    lax.fori_loop(0, heads // 2, near_inner, 0)
-    poll(guests)
-    lax.fori_loop(heads // 2, heads, near_inner, 0)
-    neighbours(0)
-    visit_first(0)
-    attend(0)
     visit_second(0)
+    for h in range(guests, heads):
+        ask(h, 0)
     for h in range(1, guests):
         poll(guests + h)
+        near_inner(guests)
         neighbours(h)
         visit_second(h)
         visit_first(h)
         attend(h)
     for h in range(2 * guests, heads):
         poll(h)
+    for h in range(guests + 1, heads):
+        near_inner(h)
     for h in range(guests):
         merge(h)
     for h in range(guests, heads):
@@ -509,8 +521,7 @@
             combine(h - guests, 0)
     for h in range(heads - guests - 1, heads - 1):
         combine(h, 0)
-    for copy in wo_copies:
-        copy.wait()
+    pltpu.make_async_copy(wo_hbm, wo, wo_sem.at[0]).wait()
     for h in range(heads - 1):
         gathered(h, 0)
     partial_out()
@@ -519,18 +530,25 @@
     gathered(heads - 1, 0)
     add_last(other, out_ref)
 
-    for i in range(PIECES):
-        x_copy(i).wait_send()
-
-    for h in range(heads):
-        sends = send_second(h) + send_back(h) + send_part(h)
-        for half in range(2):
-            sends = sends + send_down(h, half) + send_side(h, half) + send_relay(h, half) + send_query(h, half)
-        for condition, copy in sends:
-            @pl.when(condition)
-            def _():
-                copy.wait_send()
-        mix_copy(h).wait_send()
+    x_copy.wait_send()
+    firsts, rest = pl.ds(0, guests), pl.ds(guests, heads - guests)
+    for condition, ref, kind in (
+        (has_next, ctx.at[rest, :, :, O], DOWN),
+        (even, ctx.at[:, :, :, O], SIDE),
+        (odd == 1, ctx.at[firsts, :, :, O], SIDE),
+        ((odd == 1) & (z > 0), ctx.at[rest, :, :, A], RELAY),
+        (z > 0, q, ASK),
+        (has_next & (z > 0), visitor.at[firsts], SECOND),
+        (has_next, part, PART),
+        (has_next, part_lse, LSE),
+        (has_second, back, MID),
+        (has_second, back_lse, MID_LSE),
+    ):
+        @pl.when(condition)
+        def _():
+            remote(ref, ref, sent.at[kind], x_sem.at[1], side).wait_send()
+    half_mix = mixg.at[:, pl.ds(0, heads * HEAD)]
+    remote(half_mix, half_mix, sent.at[MIX], x_sem.at[1], across).wait_send()
 
 
 def body(tokens, query_weight, key_weight, value_weight, output_weight):
@@ -597,22 +615,21 @@
             pltpu.VMEM((rows, HEAD), F32),
             pltpu.VMEM((rows, 2 * heads * HEAD), BF16),
             pltpu.VMEM((rows, out_cols), F32),
-            dma((PIECES,)),
-            dma((2, heads)),
+            dma((1,)),
+            dma((1,)),
+            dma((heads,)),
             dma((heads // 2,)),
-            dma((2, heads)),
             dma((1,)),
-            dma((PIECES,)),
-            dma((PIECES,)),
-            dma((2, heads, 2)),
-            dma((2, heads, 2)),
-            dma((2, heads, 2)),
-            dma((2, guests)),
-            dma((2, heads)),
-            dma((2, heads)),
-            dma((2, guests)),
-            dma((2, guests)),
+            dma((2,)),
+            dma((10,)),
+            dma((heads - guests,)),
             dma((heads,)),
+            dma((heads + guests,)),
+            dma((guests,)),
+            dma((heads,)),
+            dma((heads,)),
+            dma((guests,)),
+            dma((guests,)),
             dma((heads,)),
         ],
         compiler_params=pltpu.CompilerParams(

time: 38.6 us -> 37.5 us (0.972)
  Pallas kernels: 37.3 us -> 36.3 us
    pallas_call x1, Pallas kernels: 37.3 us -> 36.3 us  [body(): pl.pallas_call(functools.partial(kernel, n_sp, heads, guests), out_shape=...]
where the time goes in v4:
time: 37.5 us; the launch traced here: 37.2 us
  Pallas kernels  36.3 us (97%)
  local copies, waits for them, and re-layouts  0.97 us (3%)
    pallas_call x1, Pallas kernels, body(): pl.pallas_call(functools.partial(kernel, n_sp, heads, guests), out_shape=...  36.3 us
    unnamed x1, local copies, waits for them, and re-layouts  0.97 us

profile of v4, /device:TPU:11, one launch (start us, length us, event | category | flops | bytes accessed | tf_op | source)
XLA Modules:
  0.0 37.2 jit_solution(3224136383884329325)
XLA Ops:
  0.0 36.3 %shard_map.64 = bf16[512,1024]{1,0:T(8,128)(2,1)S(1)} custom-call(bf16[256,2048]{1,0:T(8,128)(2,1)} %tok_hbm.1, bf16[2048,512]{1,0:T(8,128)(2,1)} %wq_hbm.1, bf16[2048,512]{1,0:T(8,128)(2,1)} %wk_hbm.1, bf16[2048,512]{1,0:T(8,128)(2,1)} %wv_hbm.1, bf16[1024,1024]{1,0:T(8,128)(2,1)} %wo_hbm.1, f32[1,128]{1,0:T(1,128)} %constant.2.clone.inv_hbm), custom_call_target="tpu_custom_call" | custom-call | tf_op jit(solution)/shard_map/pallas_call | solution.py:572
  36.3 1.0 %copy.8 = bf16[512,1024]{1,0:T(8,128)(2,1)} copy(bf16[512,1024]{1,0:T(8,128)(2,1)S(1)} %shard_map.64) | data formatting | bytes 2097152

commit v5 on v4

--- a/solution.py
+++ b/solution.py
@@ -51,12 +51,12 @@
 
 def kernel(
     n_sp, heads, guests,
-    tok_hbm, wq_hbm, wk_hbm, wv_hbm, wo_hbm, inv_hbm,
+    tok_hbm, wq_hbm, wk_hbm, wv_hbm, wo_hbm,
     out_ref,
-    x, wkv, wq, wo, inv, cos_ref, sin_ref, ctx, q, qn, kn, vn, visitor, second, flat_a, flat_b,
+    x, wkv, wq, wo, cos_ref, sin_ref, ctx, q, qn, kn, vn, visitor, second, flat_a, flat_b,
     far_bias, visit_bias, pair_bias, band, num, tot, top, cnum, ctot, ctop, vnum, vtot, vtop,
     part, part_lse, far_out, far_lse, back, back_lse, mid_out, mid_lse, mixf, mixg, out_sum,
-    tok_sem, inv_sem, kv_sem, q_load, wo_sem, x_sem, sent,
+    tok_sem, kv_sem, q_load, wo_sem, x_sem, sent,
     a_recv, c_recv, q_recv, second_recv, part_recv, lse_recv, mid_recv, mid_lse_recv, mix_recv,
 ):
     sp = lax.axis_index("sp")
@@ -74,8 +74,6 @@
     piece = half_rows // PIECES
     order = (tp, other)
 
-    inv_copy = pltpu.make_async_copy(inv_hbm, inv, inv_sem.at[0])
-    inv_copy.start()
     tok_copy = pltpu.make_async_copy(tok_hbm, x.at[tp], tok_sem.at[0])
     tok_copy.start()
 
@@ -170,27 +168,42 @@
             mid_lse[...] = jnp.full(mid_lse.shape, NEG, F32)
 
     lane = iota((piece, HEAD), 1)
+    low = lane < HEAD // 2
+    power = (iota((1, HEAD), 1) % (HEAD // 2)).astype(F32)
+    inverse = jnp.exp2(power * (-2.0 * float(np.log2(THETA_BASE)) / HEAD))
 
     def table(c, _):
         start = pl.multiple_of(c * piece, piece)
-        positions = sp * rows + start + iota((piece, HEAD), 0)
-        angles = positions.astype(F32) * inv[...]
-        span = pl.ds(start, piece)
-        cos_ref[span, :] = jnp.cos(angles)
-        sine = jnp.sin(angles)
-        sin_ref[span, :] = jnp.where(lane < HEAD // 2, -sine, sine)
+        places = start + iota((piece, HEAD), 0) + half_rows * jnp.where(low, tp, other)
+        angles = (sp * rows + places).astype(F32) * inverse
+        cosine, sine = jnp.cos(angles), jnp.sin(angles)
+        cosine_moved, sine_moved = pltpu.roll(cosine, HEAD // 2, 1), pltpu.roll(sine, HEAD // 2, 1)
+        own = pl.ds(pl.multiple_of(tp * half_rows + start, piece), piece)
+        rest = pl.ds(pl.multiple_of(other * half_rows + start, piece), piece)
+        cos_ref[own, :] = jnp.where(low, cosine, cosine_moved)
+        sin_ref[own, :] = jnp.where(low, -sine, sine_moved)
+        cos_ref[rest, :] = jnp.where(low, cosine_moved, cosine)
+        sin_ref[rest, :] = jnp.where(low, -sine_moved, sine)
         return 0
 
-    inv_copy.wait()
+    lax.fori_loop(0, PIECES, table, 0)
+    q_copies[0].start()
     for kind in range(2):
         kv_copy(0, kind).start()
-    q_copies[0].start()
-    lax.fori_loop(tp * PIECES, tp * PIECES + PIECES, table, 0)
+
+    def load_kv(h):
+        pltpu.make_async_copy(wk_hbm.at[:, pl.ds(0, 2 * HEAD)], wkv.at[h], kv_sem.at[h]).wait()
+
+    def raw_kv(source, h, count):
+        kv = jnp.dot(source, wkv[h], preferred_element_type=F32)
+        flat_a[0:count] = kv[:, :HEAD]
+        flat_b[0:count] = kv[:, HEAD:]
+
+    tok_copy.wait()
 
     pl.semaphore_wait(barrier, 2 + has_next.astype(jnp.int32) + (z > 0).astype(jnp.int32))
 
     x_copy = remote(x.at[tp], x.at[tp], x_sem.at[0], x_sem.at[1], across)
-    tok_copy.wait()
     x_copy.start()
     for h in (*range(guests + 1, heads), *range(1, guests)):
         for kind in range(2):
@@ -247,22 +260,18 @@
 
     def project_kv(h, half):
         if half is None:
-            source, natural, span = x[...].reshape(rows, x.shape[2]), pl.ds(0, rows), (0, rows)
-            spots = pl.ds(0, class_rows)
+            source, natural, count, spots = x[...].reshape(rows, x.shape[2]), pl.ds(0, rows), rows, every
         else:
             source, natural = x[half], pl.ds(pl.multiple_of(half * half_rows, half_rows), half_rows)
-            span, spots = (0, half_rows), pl.ds(pl.multiple_of(half * half_class, half_class), half_class)
-        kv = jnp.dot(source, wkv[h], preferred_element_type=F32)
-        k = rotated(kv[:, :HEAD], cos_ref[natural], sin_ref[natural])
-        v = kv[:, HEAD:]
-        flat_a[span[0]:span[1]] = k
-        flat_b[span[0]:span[1]] = v
+            count, spots = half_rows, spots_of(half)
+        raw_kv(source, h, count)
+        k = rotated(flat_a[0:count], cos_ref[natural], sin_ref[natural])
+        flat_a[0:count] = k
         kn[h, natural] = k.astype(BF16)
-        vn[h, natural] = v.astype(BF16)
-        count = span[1] // CLASSES
+        vn[h, natural] = flat_b[0:count].astype(BF16)
         for c in range(CLASSES):
-            ctx[h, 0, c, O, spots] = flat_a[classed(0, count, c), :].astype(BF16)
-            ctx[h, 1, c, O, spots] = flat_b[classed(0, count, c), :].astype(BF16)
+            ctx[h, 0, c, O, spots] = flat_a[classed(0, count // CLASSES, c), :].astype(BF16)
+            ctx[h, 1, c, O, spots] = flat_b[classed(0, count // CLASSES, c), :].astype(BF16)
         for part_half in (order if half is None else (half,)):
             start_all(send_down(h, part_half))
             for condition, copy in send_side(h, part_half):
@@ -298,9 +307,6 @@
             span = slice((b - 1) * block, (b + 1) * block)
             near(h, b, kn[h, span], vn[h, span], band[1])
 
-    def load_kv(h):
-        pltpu.make_async_copy(wk_hbm.at[:, pl.ds(0, 2 * HEAD)], wkv.at[h], kv_sem.at[h]).wait()
-
     def poll(h):
         @pl.when((odd == 1) & (z > 0))
         def _():
@@ -329,8 +335,7 @@
                 block_copy(h, C, C, every, SIDE, side).wait_recv()
 
     def mix_copy(h):
-        cols = pl.ds(pl.multiple_of((2 * h + tp) * HEAD, HEAD), HEAD)
-        return remote(mixg.at[:, cols], mixg.at[:, cols], sent.at[MIX], mix_recv.at[h], across)
+        return remote(mixg.at[2 * h + tp], mixg.at[2 * h + tp], sent.at[MIX], mix_recv.at[h], across)
 
     eye = iota((block, block), 0) == iota((block, block), 1)
 
@@ -421,8 +426,7 @@
         for c in range(CLASSES):
             mixed, _, _ = with_far(cnum[h, c], ctot[h, c], ctop[h, c], far_out[h, c], far_lse[h, pl.ds(c, 1), :])
             mixf[classed(0, class_rows, c), :] = mixed
-        cols = pl.ds(pl.multiple_of((2 * h + tp) * HEAD, HEAD), HEAD)
-        mixg[:, cols] = mixf[...].astype(BF16)
+        mixg[2 * h + tp] = mixf[...].astype(BF16)
         mix_copy(h).start()
         return 0
 
@@ -434,17 +438,19 @@
     wide = 256
 
     def add_last(t, into):
-        span = pl.ds(pl.multiple_of((2 * (heads - 1) + t) * HEAD, HEAD), HEAD)
+        at = 2 * (heads - 1) + t
+        span = pl.ds(pl.multiple_of(at * HEAD, HEAD), HEAD)
         for i in range(out_cols // wide):
             cols = pl.ds(i * wide, wide)
-            total = jnp.dot(mixg[:, span], wo[span, cols], preferred_element_type=F32)
+            total = jnp.dot(mixg[at], wo[span, cols], preferred_element_type=F32)
             into[:, cols] = (out_sum[:, cols] + total).astype(into.dtype)
 
     def partial_out():
-        most_in = (heads - 1) * 2 * HEAD
+        most = 2 * (heads - 1)
+        mixed = jnp.concatenate([mixg[i] for i in range(most)], axis=1)
         for i in range(out_cols // wide):
             cols = pl.ds(i * wide, wide)
-            out_sum[:, cols] = jnp.dot(mixg[:, :most_in], wo[:most_in, cols], preferred_element_type=F32)
+            out_sum[:, cols] = jnp.dot(mixed, wo[:most * HEAD, cols], preferred_element_type=F32)
 
     def ask(h, half):
         @pl.when(z > 0)
@@ -459,7 +465,6 @@
         ask(h, tp)
     load_kv(0)
     project_kv(0, tp)
-    lax.fori_loop(other * PIECES, other * PIECES + PIECES, table, 0)
     x_copy.wait_recv()
     project_kv(guests, other)
     project_q(0, other)
@@ -484,20 +489,20 @@
     meet(0, tp)
     masks()
     meet(0, other)
-    for h in range(1, guests):
-        meet(h, tp)
     near_inner(0)
     near_inner(1)
     neighbours(0)
+    for h in range(1, guests):
+        meet(h, tp)
     visit_first(0)
     for h in range(1, guests):
         meet(h, other)
     poll(guests)
     attend(0)
+    visit_second(0)
     for p in range(1, heads // 2):
         q_copies[p].wait()
         project_q(p, None)
-    visit_second(0)
     for h in range(guests, heads):
         ask(h, 0)
     for h in range(1, guests):
@@ -519,13 +524,12 @@
         attend(h)
         if h < heads - 1:
             combine(h - guests, 0)
-    for h in range(heads - guests - 1, heads - 1):
+    for h in range(heads - guests - 1, heads):
         combine(h, 0)
     pltpu.make_async_copy(wo_hbm, wo, wo_sem.at[0]).wait()
     for h in range(heads - 1):
         gathered(h, 0)
     partial_out()
-    combine(heads - 1, 0)
     add_last(tp, out_sum)
     gathered(heads - 1, 0)
     add_last(other, out_ref)
@@ -547,7 +551,7 @@
         @pl.when(condition)
         def _():
             remote(ref, ref, sent.at[kind], x_sem.at[1], side).wait_send()
-    half_mix = mixg.at[:, pl.ds(0, heads * HEAD)]
+    half_mix = mixg.at[pl.ds(0, heads)]
     remote(half_mix, half_mix, sent.at[MIX], x_sem.at[1], across).wait_send()
 
 
@@ -558,10 +562,6 @@
     heads = query_weight.shape[1] // HEAD
     assert rows * 4 == FAR_DILATION * REACH_STEPS and rows == 512
     assert n_sp % 2 == 0 and lax.axis_size("tp") == 2 and heads % 2 == 0 and heads >= 4
-
-    half = HEAD // 2
-    inverse = THETA_BASE ** (-np.arange(half, dtype=np.float64) / half)
-    inverse = np.concatenate([inverse, inverse]).astype(np.float32)[None, :]
 
     guests = heads // 2
     class_rows = rows // CLASSES
@@ -572,14 +572,13 @@
     return pl.pallas_call(
         functools.partial(kernel, n_sp, heads, guests),
         out_shape=pltpu.VMEM((rows, out_cols), BF16),
-        in_specs=[anywhere] * 6,
+        in_specs=[anywhere] * 5,
         out_specs=vmem,
         scratch_shapes=[
             pltpu.VMEM((2, half_rows, width), BF16),
             pltpu.VMEM((heads, width, 2 * HEAD), BF16),
             pltpu.VMEM((heads // 2, width, 2 * HEAD), BF16),
             pltpu.VMEM(output_weight.shape, BF16),
-            pltpu.VMEM((1, HEAD), F32),
             pltpu.VMEM((rows, HEAD), F32),
             pltpu.VMEM((rows, HEAD), F32),
             pltpu.VMEM((heads, 2, CLASSES, SLOTS, class_rows, HEAD), BF16),
@@ -613,9 +612,8 @@
             pltpu.VMEM((guests, CLASSES, class_rows, HEAD), BF16),
             pltpu.VMEM((guests, 8, 128), F32),
             pltpu.VMEM((rows, HEAD), F32),
-            pltpu.VMEM((rows, 2 * heads * HEAD), BF16),
+            pltpu.VMEM((2 * heads, rows, HEAD), BF16),
             pltpu.VMEM((rows, out_cols), F32),
-            dma((1,)),
             dma((1,)),
             dma((heads,)),
             dma((heads // 2,)),
@@ -635,7 +633,7 @@
         compiler_params=pltpu.CompilerParams(
             collective_id=0, has_side_effects=True, vmem_limit_bytes=56 * 1024 * 1024
         ),
-    )(tokens, query_weight, key_weight, value_weight, output_weight, jnp.asarray(inverse))
+    )(tokens, query_weight, key_weight, value_weight, output_weight)
 
 
 def solution(mesh):

time: 37.5 us -> 37.1 us (0.989)
  no operation moved by 1% of the time
where the time goes in v5:
time: 37.1 us; the launch traced here: 37 us
  Pallas kernels  36 us (97%)
  local copies, waits for them, and re-layouts  0.97 us (3%)
    pallas_call x1, Pallas kernels, body(): pl.pallas_call(functools.partial(kernel, n_sp, heads, guests), out_shape=...  36 us
    unnamed x1, local copies, waits for them, and re-layouts  0.97 us

profile of v5, /device:TPU:11, one launch (start us, length us, event | category | flops | bytes accessed | tf_op | source)
XLA Modules:
  0.0 37.0 jit_solution(1910684166325206129)
XLA Ops:
  0.0 36.0 %shard_map.55 = bf16[512,1024]{1,0:T(8,128)(2,1)S(1)} custom-call(bf16[256,2048]{1,0:T(8,128)(2,1)} %tok_hbm.1, bf16[2048,512]{1,0:T(8,128)(2,1)} %wq_hbm.1, bf16[2048,512]{1,0:T(8,128)(2,1)} %wk_hbm.1, bf16[2048,512]{1,0:T(8,128)(2,1)} %wv_hbm.1, bf16[1024,1024]{1,0:T(8,128)(2,1)} %wo_hbm.1), custom_call_target="tpu_custom_call" | custom-call | tf_op jit(solution)/shard_map/pallas_call | solution.py:572
  36.0 1.0 %copy.7 = bf16[512,1024]{1,0:T(8,128)(2,1)} copy(bf16[512,1024]{1,0:T(8,128)(2,1)S(1)} %shard_map.55) | data formatting | bytes 2097152

commit v6 on v5

--- a/solution.py
+++ b/solution.py
@@ -57,7 +57,7 @@
     far_bias, visit_bias, pair_bias, band, num, tot, top, cnum, ctot, ctop, vnum, vtot, vtop,
     part, part_lse, far_out, far_lse, back, back_lse, mid_out, mid_lse, mixf, mixg, out_sum,
     tok_sem, kv_sem, q_load, wo_sem, x_sem, sent,
-    a_recv, c_recv, q_recv, second_recv, part_recv, lse_recv, mid_recv, mid_lse_recv, mix_recv,
+    a_recv, c_recv, q_recv, second_recv, part_recv, mid_recv, mix_recv,
 ):
     sp = lax.axis_index("sp")
     tp = lax.axis_index("tp")
@@ -211,7 +211,12 @@
     for copy in (*q_copies[1:], *wo_copies):
         copy.start()
 
-    DOWN, SIDE, RELAY, ASK, SECOND, PART, LSE, MID, MID_LSE, MIX = range(10)
+    DOWN, SIDE, RELAY, ASK, SECOND, PART, MID, MIX = range(8)
+    result_rows = (CLASSES * class_rows * HEAD // 2 + part_lse.shape[1] * HEAD) // HEAD
+
+    def results(count, kind, arrived):
+        both = num.at[pl.ds(0, count * result_rows)]
+        return remote(both, both, sent.at[kind], arrived, down)
 
     def spots_of(half):
         return pl.ds(pl.multiple_of(half * half_class, half_class), half_class)
@@ -240,11 +245,11 @@
 
     def back_copies(h):
         return (remote(back.at[h], mid_out.at[h], sent.at[MID], mid_recv.at[h], down),
-                remote(back_lse.at[h], mid_lse.at[h], sent.at[MID_LSE], mid_lse_recv.at[h], down))
+                remote(back_lse.at[h], mid_lse.at[h], sent.at[MID], mid_recv.at[h], down))
 
     def part_copies(h):
         return (remote(part.at[h], far_out.at[h], sent.at[PART], part_recv.at[h], down),
-                remote(part_lse.at[h], far_lse.at[h], sent.at[LSE], lse_recv.at[h], down))
+                remote(part_lse.at[h], far_lse.at[h], sent.at[PART], part_recv.at[h], down))
 
     def send_back(h):
         return tuple((has_second, copy) for copy in back_copies(h))
@@ -335,7 +340,7 @@
                 block_copy(h, C, C, every, SIDE, side).wait_recv()
 
     def mix_copy(h):
-        return remote(mixg.at[2 * h + tp], mixg.at[2 * h + tp], sent.at[MIX], mix_recv.at[h], across)
+        return remote(mixg.at[2 * h + tp], mixg.at[2 * h + tp], sent.at[MIX], mix_recv.at[(h + 1) // heads], across)
 
     eye = iota((block, block), 0) == iota((block, block), 1)
 
@@ -398,8 +403,7 @@
         def _():
             @pl.when(z > 0)
             def _():
-                for copy in back_copies(h):
-                    copy.wait_recv()
+                results(1, MID, mid_recv.at[h]).wait_recv()
             for c in range(CLASSES):
                 r, t, m = with_far(vnum[h, c], vtot[h, c], vtop[h, c], mid_out[h, c], mid_lse[h, c:c + 1, :])
                 part[h, c] = r.astype(BF16)
@@ -420,8 +424,7 @@
     def combine(h, _):
         @pl.when(z > 0)
         def _():
-            for copy in part_copies(h):
-                copy.wait_recv()
+            results(1, PART, part_recv.at[h]).wait_recv()
 
         for c in range(CLASSES):
             mixed, _, _ = with_far(cnum[h, c], ctot[h, c], ctop[h, c], far_out[h, c], far_lse[h, pl.ds(c, 1), :])
@@ -430,9 +433,9 @@
         mix_copy(h).start()
         return 0
 
-    def gathered(h, _):
-        mix_copy(h).wait_recv()
-        return 0
+    def gathered(count, which):
+        some = mixg.at[pl.ds(0, count)]
+        remote(some, some, sent.at[MIX], mix_recv.at[which], across).wait_recv()
 
     out_cols = out_ref.shape[1]
     wide = 256
@@ -527,11 +530,10 @@
     for h in range(heads - guests - 1, heads):
         combine(h, 0)
     pltpu.make_async_copy(wo_hbm, wo, wo_sem.at[0]).wait()
-    for h in range(heads - 1):
-        gathered(h, 0)
+    gathered(heads - 1, 0)
     partial_out()
     add_last(tp, out_sum)
-    gathered(heads - 1, 0)
+    gathered(1, 1)
     add_last(other, out_ref)
 
     x_copy.wait_send()
@@ -543,10 +545,8 @@
         ((odd == 1) & (z > 0), ctx.at[rest, :, :, A], RELAY),
         (z > 0, q, ASK),
         (has_next & (z > 0), visitor.at[firsts], SECOND),
-        (has_next, part, PART),
-        (has_next, part_lse, LSE),
-        (has_second, back, MID),
-        (has_second, back_lse, MID_LSE),
+        (has_next, num.at[pl.ds(0, heads * result_rows)], PART),
+        (has_second, num.at[pl.ds(0, guests * result_rows)], MID),
     ):
         @pl.when(condition)
         def _():
@@ -619,16 +619,14 @@
             dma((heads // 2,)),
             dma((1,)),
             dma((2,)),
-            dma((10,)),
+            dma((8,)),
             dma((heads - guests,)),
             dma((heads,)),
             dma((heads + guests,)),
             dma((guests,)),
             dma((heads,)),
-            dma((heads,)),
             dma((guests,)),
-            dma((guests,)),
-            dma((heads,)),
+            dma((2,)),
         ],
         compiler_params=pltpu.CompilerParams(
             collective_id=0, has_side_effects=True, vmem_limit_bytes=56 * 1024 * 1024

time: 37.1 us -> 37 us (level)
  no operation moved by 1% of the time
where the time goes in v6:
time: 37 us; the launch traced here: 36.9 us
  Pallas kernels  35.9 us (97%)
  local copies, waits for them, and re-layouts  0.97 us (3%)
    pallas_call x1, Pallas kernels, body(): pl.pallas_call(functools.partial(kernel, n_sp, heads, guests), out_shape=...  35.9 us
    unnamed x1, local copies, waits for them, and re-layouts  0.97 us

profile of v6, /device:TPU:11, one launch (start us, length us, event | category | flops | bytes accessed | tf_op | source)
XLA Modules:
  0.0 36.9 jit_solution(16244581012819313535)
XLA Ops:
  0.0 35.9 %shard_map.55 = bf16[512,1024]{1,0:T(8,128)(2,1)S(1)} custom-call(bf16[256,2048]{1,0:T(8,128)(2,1)} %tok_hbm.1, bf16[2048,512]{1,0:T(8,128)(2,1)} %wq_hbm.1, bf16[2048,512]{1,0:T(8,128)(2,1)} %wk_hbm.1, bf16[2048,512]{1,0:T(8,128)(2,1)} %wv_hbm.1, bf16[1024,1024]{1,0:T(8,128)(2,1)} %wo_hbm.1), custom_call_target="tpu_custom_call" | custom-call | tf_op jit(solution)/shard_map/pallas_call | solution.py:572
  35.9 1.0 %copy.7 = bf16[512,1024]{1,0:T(8,128)(2,1)} copy(bf16[512,1024]{1,0:T(8,128)(2,1)S(1)} %shard_map.55) | data formatting | bytes 2097152

commit v7 on v6

--- a/solution.py
+++ b/solution.py
@@ -469,9 +469,9 @@
     load_kv(0)
     project_kv(0, tp)
     x_copy.wait_recv()
-    project_kv(guests, other)
     project_q(0, other)
     ask(0, other)
+    project_kv(guests, other)
     project_kv(0, other)
 
     def project_rest(i, _):

time: 37 us -> 37 us (level)
  no operation moved by 1% of the time
where the time goes in v7:
time: 37 us; the launch traced here: 36.9 us
  Pallas kernels  35.9 us (97%)
  local copies, waits for them, and re-layouts  0.97 us (3%)
    pallas_call x1, Pallas kernels, body(): pl.pallas_call(functools.partial(kernel, n_sp, heads, guests), out_shape=...  35.9 us
    unnamed x1, local copies, waits for them, and re-layouts  0.97 us

profile of v7, /device:TPU:11, one launch (start us, length us, event | category | flops | bytes accessed | tf_op | source)
XLA Modules:
  0.0 36.9 jit_solution(14389866819873791862)
XLA Ops:
  0.0 35.9 %shard_map.55 = bf16[512,1024]{1,0:T(8,128)(2,1)S(1)} custom-call(bf16[256,2048]{1,0:T(8,128)(2,1)} %tok_hbm.1, bf16[2048,512]{1,0:T(8,128)(2,1)} %wq_hbm.1, bf16[2048,512]{1,0:T(8,128)(2,1)} %wk_hbm.1, bf16[2048,512]{1,0:T(8,128)(2,1)} %wv_hbm.1, bf16[1024,1024]{1,0:T(8,128)(2,1)} %wo_hbm.1), custom_call_target="tpu_custom_call" | custom-call | tf_op jit(solution)/shard_map/pallas_call | solution.py:572
  35.9 1.0 %copy.7 = bf16[512,1024]{1,0:T(8,128)(2,1)} copy(bf16[512,1024]{1,0:T(8,128)(2,1)S(1)} %shard_map.55) | data formatting | bytes 2097152
